TPU v7x, 32 devices: a whole 2x2x4 slice. The times are simulated.
32 devices in a mesh: grp: 2 (over x), st: 4 (over y, core), tp: 4 (over z).
Axes of the slice: x: 2, y: 2, z: 4, core: 2. Of those that a mesh axis runs over, the one named last changes fastest.
Arguments:
- tokens: bfloat16 [4096, 2048], P(('grp', 'st')), parts along dimension 0, may hold values from -6 to 6, as said below
- store: bfloat16 [64, 128, 2048], P(('grp', 'st')), parts along dimension 0, may hold values from -6 to 6, as said below
- passage_ids: int32 [64, 4], P(('grp', 'st')), parts along dimension 0, may hold values from 0 to 31, as said below
- mix_gain: float32 [2048], replicated, may hold values from 0.1 to 1.9
- glu_value: bfloat16 [2048, 1024], P(None, 'tp'), may hold values from -0.125 to 0.125
- glu_gate: bfloat16 [2048, 1024], P(None, 'tp'), may hold values from -0.125 to 0.125
- conv_taps: bfloat16 [31, 1024], P(None, 'tp'), may hold values from -5 to 5
- channel_gain: float32 [1024], P('tp'), may hold values from 0.1 to 1.9
- mix_out: bfloat16 [1024, 2048], P('tp'), may hold values from -0.1875 to 0.1875
- query_gain: float32 [2048], replicated, may hold values from 0.1 to 1.9
- passage_gain: float32 [2048], replicated, may hold values from 0.1 to 1.9
- query_proj: bfloat16 [2048, 2048], P(None, 'tp'), may hold values from -1 to 1
- key_proj: bfloat16 [2048, 2048], P(None, 'tp'), may hold values from -1 to 1
- value_proj: bfloat16 [2048, 2048], P(None, 'tp'), may hold values from -0.125 to 0.125
- attn_out: bfloat16 [2048, 2048], P('tp'), may hold values from -0.125 to 0.125
- blend_gain: float32 [2048], replicated, may hold values from 0.5 to 3
Outputs:
- blended: bfloat16 [4096, 2048], P(('grp', 'st', 'tp')), parts along dimension 0
There are 2 independent parts, one for each index of `grp`. A program takes and returns all parts, laid end to end along the dimension named above; an argument that names none is the same for every part. Nothing has to cross between parts.
Inputs may be any that keep to these rules, and one draw needn't show every extreme that they name: `tokens`: standard normal entries clipped to the range. `store`: standard normal entries clipped to the range. `passage_ids`: passage p is held by index p // 8 of st. The 32 requests of the 8 blocks of one index of st (repeats counted) name at most 16 passages held by any one index of st, and in every draw one index of st receives exactly 16 requests from every index of st.
All inputs are finite; a program needn't handle non-finite values.
Results may differ from a plain program's by a relative error of at most 0.01575.
The roundings to bfloat16 on the way count: a program that leaves them out, or rounds other values in their place, can miss the bound.
Values may be sent and summed in bfloat16 or wider, within the bound.
No kernel may reach another device: no remote copies, remote signals or barrier semaphores. Data moves between devices by JAX's collectives and lax.ppermute only.
A program may use at most 128 MiB of HBM per device.

v0:
```python
import jax
import jax.numpy as jnp
from jax import lax
from jax.sharding import PartitionSpec as P

CA = 1024
HD = 256
SEQ_LEN = 128


EPS = 1e-06


def rms_rows(row_data, gain_vec):
    floats = row_data.astype(jnp.float32)
    inv_scale = lax.rsqrt(jnp.mean(floats * floats, axis=-1, keepdims=True) + EPS)
    return (floats * inv_scale * gain_vec).astype(jnp.bfloat16)


def depthwise(gated_rows, conv_taps):
    span_width = conv_taps.shape[0]
    half_span = (span_width - 1) // 2
    seq_length = gated_rows.shape[1]
    padded = jnp.pad(
        gated_rows.astype(jnp.float32), ((0, 0), (half_span, span_width - 1 - half_span), (0, 0))
    )
    running = jnp.zeros(gated_rows.shape, jnp.float32)
    for tap_index in range(span_width):
        running = running + padded[:, tap_index : tap_index + seq_length] * conv_taps[
            tap_index
        ].astype(jnp.float32)
    return running


def passage_attention(queries, keys_values, head_count):
    groups, block_len, span_width = queries.shape
    head_dim = span_width // head_count
    row_count = keys_values.shape[1]
    query_heads = queries.reshape(groups, block_len, head_count, head_dim)
    key_heads = keys_values[:, :, :span_width].reshape(groups, row_count, head_count, head_dim)
    value_heads = keys_values[:, :, span_width:].reshape(groups, row_count, head_count, head_dim)
    scores = jnp.einsum(
        "gqhd,grhd->ghqr", query_heads, key_heads, preferred_element_type=jnp.float32
    ) * head_dim ** (-0.5)
    row_top = jnp.max(scores, axis=-1)
    exponent = jnp.exp(scores - row_top[..., None])
    row_sum = jnp.sum(exponent, axis=-1)
    weights = exponent.astype(jnp.bfloat16)
    outputs = jnp.einsum(
        "ghqr,grhd->gqhd", weights, value_heads, preferred_element_type=jnp.float32
    ).astype(jnp.bfloat16)
    return (outputs.reshape(groups, block_len, span_width), row_top, row_sum)


def combine(outs, tops, sums, head_count):
    batch_count, passage_count, block_len, span_width = outs.shape
    head_dim = span_width // head_count
    best_top = jnp.max(tops, axis=1, keepdims=True)
    weight = jnp.exp(tops - best_top)
    numerator = jnp.einsum(
        "bphq,bpqhd->bqhd",
        weight,
        outs.astype(jnp.float32).reshape(
            batch_count, passage_count, block_len, head_count, head_dim
        ),
    )
    denominator = jnp.sum(weight * sums, axis=1)
    result = numerator / jnp.transpose(denominator, (0, 2, 1))[..., None]
    return result.reshape(batch_count, block_len, span_width).astype(jnp.bfloat16)


def local(
    tokens,
    store,
    passage_ids,
    mix_gain,
    glu_value,
    glu_gate,
    conv_taps,
    channel_gain,
    mix_out,
    query_gain,
    passage_gain,
    query_proj,
    key_proj,
    value_proj,
    attn_out,
    blend_gain,
):
    owners = lax.axis_size("st")
    tok_rows = tokens.shape[0]
    model_width = tokens.shape[1]
    local_channels = glu_value.shape[1]
    head_width = query_proj.shape[1]
    local_heads = head_width // HD
    block_count = passage_ids.shape[0]
    per_block = passage_ids.shape[1]
    block_len = tok_rows // block_count
    requests = block_count * per_block
    capacity = 2 * requests // owners
    pass_local = store.shape[0]
    pass_rows = store.shape[1]
    flat_ids = passage_ids.reshape(requests)
    owner_of = flat_ids // pass_local
    local_of = flat_ids - owner_of * pass_local
    request_index = jnp.arange(requests)
    earlier = (owner_of[:, None] == owner_of[None, :]) & (
        request_index[None, :] < request_index[:, None]
    )
    ranking = jnp.sum(earlier.astype(jnp.int32), axis=1)
    slot_of = owner_of * capacity + ranking
    slot_ids = (
        jnp.zeros((owners * capacity,), jnp.int32)
        .at[slot_of]
        .set(local_of)
        .reshape(owners, capacity)
    )
    asked = lax.all_to_all(slot_ids, "st", split_axis=0, concat_axis=0, tiled=True)
    normed_store = rms_rows(store.reshape(pass_local * pass_rows, model_width), passage_gain)
    key_rows = jnp.dot(normed_store, key_proj, preferred_element_type=jnp.float32).astype(
        jnp.bfloat16
    )
    value_rows = jnp.dot(normed_store, value_proj, preferred_element_type=jnp.float32).astype(
        jnp.bfloat16
    )
    memory = jnp.concatenate([key_rows, value_rows], axis=1).reshape(
        pass_local, pass_rows, 2 * head_width
    )
    queries = jnp.dot(
        rms_rows(tokens, query_gain), query_proj, preferred_element_type=jnp.float32
    ).astype(jnp.bfloat16)
    query_blocks = queries.reshape(block_count, block_len, head_width)
    repeated = jnp.repeat(query_blocks, per_block, axis=0)
    served = memory[asked.reshape(owners * capacity)]
    slot_queries = (
        jnp.zeros((owners * capacity, block_len, head_width), jnp.bfloat16)
        .at[slot_of]
        .set(repeated)
    )
    visiting = lax.all_to_all(
        slot_queries.reshape(owners, capacity, block_len, head_width),
        "st",
        split_axis=0,
        concat_axis=0,
        tiled=True,
    )
    answer_out, answer_top, answer_sum = passage_attention(
        visiting.reshape(owners * capacity, block_len, head_width), served, local_heads
    )
    back_out = lax.all_to_all(
        answer_out.reshape(owners, capacity, block_len, head_width),
        "st",
        split_axis=0,
        concat_axis=0,
        tiled=True,
    )
    back_top, back_sum = (
        lax.all_to_all(
            answer_top.reshape(owners, capacity, local_heads, block_len),
            "st",
            split_axis=0,
            concat_axis=0,
            tiled=True,
        ),
        lax.all_to_all(
            answer_sum.reshape(owners, capacity, local_heads, block_len),
            "st",
            split_axis=0,
            concat_axis=0,
            tiled=True,
        ),
    )
    partial_out = back_out.reshape(owners * capacity, block_len, head_width)[slot_of]
    partial_top = back_top.reshape(owners * capacity, local_heads, block_len)[slot_of]
    partial_sum = back_sum.reshape(owners * capacity, local_heads, block_len)[slot_of]
    attended = combine(
        partial_out.reshape(block_count, per_block, block_len, head_width),
        partial_top.reshape(block_count, per_block, local_heads, block_len),
        partial_sum.reshape(block_count, per_block, local_heads, block_len),
        local_heads,
    ).reshape(tok_rows, head_width)
    mix_input = rms_rows(tokens, mix_gain)
    value_part = jnp.dot(mix_input, glu_value, preferred_element_type=jnp.float32)
    gate_part = jnp.dot(mix_input, glu_gate, preferred_element_type=jnp.float32)
    gated_rows = (value_part * jax.nn.sigmoid(gate_part)).astype(jnp.bfloat16)
    conv_rows = depthwise(gated_rows.reshape(-1, SEQ_LEN, local_channels), conv_taps).reshape(
        tok_rows, local_channels
    )
    channel_sum, channel_square = lax.psum(
        (jnp.sum(conv_rows, axis=1), jnp.sum(conv_rows * conv_rows, axis=1)), "tp"
    )
    row_mean = channel_sum / CA
    row_var = channel_square / CA - row_mean * row_mean
    activation = jax.nn.silu(
        (conv_rows - row_mean[:, None]) * lax.rsqrt(row_var + EPS)[:, None] * channel_gain
    ).astype(jnp.bfloat16)
    conv_term = jnp.dot(activation, mix_out, preferred_element_type=jnp.float32)
    attn_term = jnp.dot(attended, attn_out, preferred_element_type=jnp.float32)
    return lax.psum_scatter(
        (conv_term + blend_gain * attn_term).astype(jnp.bfloat16),
        "tp",
        scatter_dimension=0,
        tiled=True,
    )


def solution(mesh):
    in_specs = (
        P(("grp", "st"), None),
        P(("grp", "st"), None, None),
        P(("grp", "st"), None),
        P(),
        P(None, "tp"),
        P(None, "tp"),
        P(None, "tp"),
        P("tp"),
        P("tp", None),
        P(),
        P(),
        P(None, "tp"),
        P(None, "tp"),
        P(None, "tp"),
        P("tp", None),
        P(),
    )
    out_specs = P(("grp", "st", "tp"), None)
    return jax.shard_map(local, mesh=mesh, in_specs=in_specs, out_specs=out_specs, check_vma=False)
```

profile of v0, /device:TPU:9, one launch (start us, length us, event | category | flops | bytes accessed | tf_op | source)
XLA Modules:
  0.0 265.1 jit_solution(15184894235322269464)
XLA Ops:
  6.5 0.9 copy.39
  7.8 0.7 scatter_custom_fusion.1
  8.5 0.7 all_to_all.19
  9.2 3.9 %all-to-all-start.1 = ((s32[4,1,16]{2,1,0:T(1,128)}), s32[4,1,16]{2,1,0:T(1,128)S(1)}, u32[]{:S(2)}, u32[]{:S(2)}) async-start(s32[4,1,16]{2,1,0:T(1,128)} %bitcast.44), calls=%async_computation.1 | async-start | bytes 4096 | tf_op jit(solution)/shard_map/all_to_all | solution.py:118
  13.0 3.2 %multiply_reduce_fusion = f32[8,128]{1,0:T(8,128)S(1)} fusion(bf16[8,128,2048]{2,1,0:T(8,128)(2,1)} %param.17), kind=kLoop, calls=%fused_computation.9 | loop fusion | flops 6290432 | bytes 4198400 | tf_op jit(solution)/shard_map/reduce_sum | solution.py:16
  16.3 2.1 fusion.6
  18.4 2.9 %fusion.1 = bf16[1024,2048]{1,0:T(8,128)(2,1)} fusion(f32[2048]{0:T(1024)S(1)} %copy-done.8, f32[1024]{0:T(1024)S(1)} %rsqrt_bitcast_fusion, bf16[8,128,2048]{2,1,0:T(8,128)(2,1)S(1)} %copy-done.2), kind=kLoop, calls=%fused_computation.8 | loop fusion | flops 8388608 | bytes 8400896 | tf_op jit(solution)/shard_map/convert_element_type | solution.py:17
  21.4 1.3 fusion.20
  22.7 1.6 broadcast_in_dim.5
  24.3 2.5 broadcast_in_dim.4
  26.7 6.2 %scatter_fusion = bf16[64,64,512]{2,1,0:T(8,128)(2,1)} fusion(bf16[64,64,512]{2,1,0:T(8,128)(2,1)} %broadcast_in_dim.4, s32[32]{0:T(128)S(1)} %fusion.95, bf16[32,64,512]{2,1,0:T(8,128)(2,1)} %bitcast.117), kind=kCustom, calls=%fused_computation.4 | custom fusion | bytes 6291584 | tf_op jit(solution)/shard_map/scatter | solution.py:138
  33.0 5.0 %all-to-all-start = ((bf16[4,16,64,512]{3,2,1,0:T(8,128)(2,1)}), bf16[4,16,64,512]{3,2,1,0:T(8,128)(2,1)}, u32[]{:S(2)}, u32[]{:S(2)}) async-start(bf16[4,16,64,512]{3,2,1,0:T(8,128)(2,1)} %bitcast.116), calls=%async_computation | async-start | bytes 8388608 | tf_op jit(solution)/shard_map/all_to_all | solution.py:140
  38.0 5.4 %convolution_convert_fusion = bf16[1024,512]{0,1:T(8,128)(2,1)S(1)} fusion(bf16[1024,2048]{1,0:T(8,128)(2,1)} %fusion.1, bf16[2048,512]{1,0:T(8,128)(2,1)} %param.29), kind=kOutput, calls=%fused_computation.33 | convolution fusion | flops 2148007936 | bytes 7340032 | tf_op jit(solution)/shard_map/dot_general | solution.py:123
  43.4 2.4 convolution_convert_fusion.1
  45.9 1.5 pad_maximum_fusion
  47.3 4.0 %copy.55 = bf16[1024,1024]{1,0:T(8,128)(2,1)} copy(bf16[1024,1024]{0,1:T(8,128)(2,1)} %pad_maximum_fusion) | data formatting | bytes 4194304 | tf_op jit(solution)/shard_map/reshape | solution.py:126
  51.8 0.7 reduce.6
  52.6 8.9 %gather_fusion = bf16[64,128,1024]{2,1,0:T(8,128)(2,1)} fusion(bf16[8,128,1024]{2,1,0:T(8,128)(2,1)} %bitcast.113, s32[1024]{0:T(1024)S(1)} %pad_clamp_fusion.1), kind=kCustom, calls=%fused_computation | custom fusion | bytes 33554688 | tf_op jit(solution)/shard_map/gather | solution.py:134
  61.5 11.6 %fusion.102 = (bf16[64,128,512]{2,1,0:T(8,128)(2,1)}, bf16[64,128,512]{2,1,0:T(8,128)(2,1)}) fusion(bf16[64,128,1024]{2,1,0:T(8,128)(2,1)} %gather_fusion), kind=kLoop, calls=%fused_computation.202 | loop fusion | bytes 33554432 | tf_op jit(solution)/shard_map/slice | solution.py:41
  73.0 11.9 %copy.43 = bf16[64,128,512]{1,2,0:T(8,128)(2,1)} copy(bf16[64,128,512]{2,1,0:T(8,128)(2,1)} %get-tuple-element.13) | data formatting | bytes 16777216 | tf_op jit(solution)/shard_map/slice | solution.py:40
  84.9 11.9 %copy.46 = bf16[64,128,512]{1,2,0:T(8,128)(2,1)} copy(bf16[64,128,512]{2,1,0:T(8,128)(2,1)} %get-tuple-element.12) | data formatting | bytes 16777216 | tf_op jit(solution)/shard_map/slice | solution.py:41
  96.8 6.9 %reshape_reshape.6 = bf16[64,64,2,256]{3,2,1,0:T(2,128)(2,1)} reshape(bf16[4,16,64,512]{3,2,1,0:T(8,128)(2,1)} %all-to-all-done) | data formatting | bytes 8388608 | tf_op jit(solution)/shard_map/reshape;reshape | solution.py:39
  103.7 8.0 %multiply_reduce_fusion.1 = (f32[64,2,64]{2,1,0:T(2,128)S(1)}, f32[64,2,64,128]{3,2,1,0:T(8,128)}) fusion(bf16[64,128,2,256]{1,3,2,0:T(8,128)(2,1)} %bitcast.115, bf16[64,64,2,256]{3,2,1,0:T(2,128)(2,1)} %reshape_reshape.6), kind=kOutput, calls=%fused_computation.22 | convolution fusion | flops 538959872 | bytes 16809984 | tf_op jit(solution)/shard_map/gqhd,grhd->ghqr/dot_general | solution.py:42
  111.7 0.7 reshape.590
  112.4 3.4 %all-to-all-start.2 = ((f32[4,1,2048]{2,1,0:T(1,128)}), f32[4,1,2048]{2,1,0:T(1,128)S(1)}, u32[]{:S(2)}, u32[]{:S(2)}) async-start(f32[4,1,2048]{2,1,0:T(1,128)} %reshape.590), calls=%async_computation.2 | async-start | bytes 65536 | tf_op jit(solution)/shard_map/all_to_all | solution.py:158
  115.8 4.0 %fusion.9 = f32[64,2,64]{2,1,0:T(2,128)S(1)} fusion(f32[64,2,64,128]{3,2,1,0:T(8,128)} %get-tuple-element.48, f32[64,2,64]{2,1,0:T(2,128)S(1)} %get-tuple-element.47), kind=kLoop, calls=%fused_computation.23 | loop fusion | flops 3137536 | bytes 4259840 | tf_op jit(solution)/shard_map/reduce_sum | solution.py:47
  119.8 0.7 reshape.592
  120.5 3.5 %all-to-all-start.4 = ((f32[4,1,2048]{2,1,0:T(1,128)}), f32[4,1,2048]{2,1,0:T(1,128)S(1)}, u32[]{:S(2)}, u32[]{:S(2)}) async-start(f32[4,1,2048]{2,1,0:T(1,128)} %reshape.592), calls=%async_computation.4 | async-start | bytes 65536 | tf_op jit(solution)/shard_map/all_to_all | solution.py:165
  124.0 10.1 %convert_bitcast_fusion = bf16[64,64,2,256]{3,1,2,0:T(8,128)(2,1)S(1)} fusion(bf16[64,128,2,256]{1,3,2,0:T(8,128)(2,1)} %bitcast.114, f32[64,2,64,128]{3,2,1,0:T(8,128)} %get-tuple-element.48, f32[64,2,64]{2,1,0:T(2,128)S(1)} %get-tuple-element.47), kind=kOutput, calls=%fused_computation.20 | convolution fusion | flops 542113792 | bytes 16809984 | tf_op jit(solution)/shard_map/ghqr,grhd->gqhd/dot_general | solution.py:49
  134.1 6.3 %copy.48 = bf16[64,64,2,256]{3,2,1,0:T(2,128)(2,1)} copy(bf16[64,64,2,256]{3,1,2,0:T(8,128)(2,1)S(1)} %convert_bitcast_fusion) | data formatting | bytes 8388608 | tf_op jit(solution)/shard_map/convert_element_type | solution.py:51
  140.4 7.6 %reshape_reshape.7 = bf16[4,16,64,512]{3,2,1,0:T(8,128)(2,1)} reshape(bf16[64,64,2,256]{3,2,1,0:T(2,128)(2,1)} %copy.48) | data formatting | bytes 8388608 | tf_op jit(solution)/shard_map/reshape;reshape | solution.py:151
  148.0 5.1 %all-to-all-start.3 = ((bf16[4,16,64,512]{3,2,1,0:T(8,128)(2,1)}), bf16[4,16,64,512]{3,2,1,0:T(8,128)(2,1)}, u32[]{:S(2)}, u32[]{:S(2)}) async-start(bf16[4,16,64,512]{3,2,1,0:T(8,128)(2,1)} %reshape_reshape.7), calls=%async_computation.3 | async-start | bytes 8388608 | tf_op jit(solution)/shard_map/all_to_all | solution.py:150
  153.2 2.8 %fusion.25 = f32[512,256]{1,0:T(8,128)S(1)} fusion(bf16[2048,256]{1,0:T(8,128)(2,1)} %param.21, bf16[512,2048]{1,0:T(8,128)(2,1)} %param.16, f32[2048]{0:T(1024)S(1)} %copy-done.14, f32[512]{0:T(512)S(1)} %add_rsqrt_fusion.1), kind=kOutput, calls=%fused_computation.70 | convolution fusion | flops 541458432 | bytes 3680256 | tf_op jit(solution)/shard_map/dot_general | solution.py:184
  156.1 0.8 bitcast_convert_fusion
  156.8 2.4 fusion.100
  159.2 7.6 %all-reduce.1 = (f32[512]{0:T(512)S(1)}, f32[512]{0:T(512)S(1)}) all-reduce(f32[512]{0:T(512)S(1)} %bitcast.127, f32[512]{0:T(512)S(1)} %bitcast.126), channel_id=1, replica_groups=mesh['grp'=2,'st'=4,'tp'=4] {'tp'}, use_global_device_ids=true, to_apply=%region_4.5 | all-reduce | flops 1024 | bytes 8192 | tf_op jit(solution)/shard_map/psum | solution.py:189
  167.1 3.9 %fusion.103 = f32[512,2048]{1,0:T(8,128)} fusion(bf16[512,256]{1,0:T(8,128)(2,1)S(1)} %multiply_convert_fusion, bf16[256,2048]{1,0:T(8,128)(2,1)} %param.24), kind=kOutput, calls=%fused_computation.204 | convolution fusion | flops 536870912 | bytes 5505024 | tf_op jit(solution)/shard_map/dot_general | solution.py:197
  171.5 0.7 reduce.7
  172.4 0.6 gather_fusion.1
  173.5 0.7 reduce.8
  174.3 0.6 gather_fusion.3
  175.1 25.4 %all-to-all-done.3 = bf16[4,16,64,512]{3,2,1,0:T(8,128)(2,1)} async-done(((bf16[4,16,64,512]{3,2,1,0:T(8,128)(2,1)}), bf16[4,16,64,512]{3,2,1,0:T(8,128)(2,1)}, u32[]{:S(2)}, u32[]{:S(2)}) %all-to-all-start.3) | async-done | bytes 4194336 | tf_op jit(solution)/shard_map/all_to_all | solution.py:150
  200.6 4.2 %gather_fusion.2 = bf16[32,64,512]{2,1,0:T(8,128)(2,1)} fusion(bf16[64,64,512]{2,1,0:T(8,128)(2,1)} %bitcast.53, s32[1024]{0:T(1024)S(1)} %pad_clamp_fusion), kind=kCustom, calls=%fused_computation.2 | custom fusion | bytes 4194432 | tf_op jit(solution)/shard_map/gather | solution.py:173
  204.8 4.0 %reshape.492 = bf16[8,4,64,2,256]{4,3,2,1,0:T(2,128)(2,1)} reshape(bf16[32,64,512]{2,1,0:T(8,128)(2,1)} %gather_fusion.2) | data formatting | bytes 4194304 | tf_op jit(solution)/shard_map/reshape | solution.py:63
  208.8 3.7 %fusion.18 = f32[8,64,2,1,256]{4,3,2,1,0:T(1,128)S(1)} fusion(bf16[8,4,2,64,1]{1,4,2,3,0:T(2,128)(2,1)S(1)} %copy.52, bf16[8,4,64,2,256]{4,3,2,1,0:T(2,128)(2,1)} %reshape.492), kind=kOutput, calls=%fused_computation.31 | convolution fusion | flops 2097152 | bytes 3153920 | tf_op jit(solution)/shard_map/bphq,bpqhd->bqhd/dot_general | solution.py:60
  212.5 0.7 fusion.27
  213.3 2.7 %add_convert_fusion = bf16[512,2048]{1,0:T(8,128)(2,1)} fusion(f32[512,2048]{1,0:T(8,128)S(1)} %copy-done.1, bf16[512,512]{1,0:T(8,128)(2,1)S(1)} %bitcast.118, bf16[512,2048]{1,0:T(8,128)(2,1)S(1)} %copy-done, f32[2048]{0:T(1024)S(1)} %copy-done.7), kind=kOutput, calls=%fused_computation.19 | convolution fusion | flops 1076887552 | bytes 8921088 | tf_op jit(solution)/shard_map/dot_general | solution.py:198
  216.0 42.2 %reduce-scatter.2.cloned.1.call-done = bf16[128,2048]{1,0:T(8,128)(2,1)} async-done(((bf16[512,2048]{1,0:T(8,128)(2,1)}), bf16[128,2048]{1,0:T(8,128)(2,1)}) %reduce-scatter.2.cloned.1.call-update) | async-done | bytes 524304 | tf_op jit(solution)/shard_map/reduce_scatter | solution.py:199
  (61 shorter events, 2.9 us)
Async XLA Ops:
  6.5 206.7 %copy-start = (bf16[512,2048]{1,0:T(8,128)(2,1)S(1)}, bf16[512,2048]{1,0:T(8,128)(2,1)}, u32[]{:S(2)}) copy-start(bf16[512,2048]{1,0:T(8,128)(2,1)} %param.30) | copy-start | bytes 6291460
  6.5 11.8 %copy-start.8 = (f32[2048]{0:T(1024)S(1)}, f32[2048]{0:T(1024)}, u32[]{:S(2)}) copy-start(f32[2048]{0:T(1024)} %param.26) | copy-start | bytes 24580
  9.2 23.8 %all-to-all-start.1 = ((s32[4,1,16]{2,1,0:T(1,128)}), s32[4,1,16]{2,1,0:T(1,128)S(1)}, u32[]{:S(2)}, u32[]{:S(2)}) async-start(s32[4,1,16]{2,1,0:T(1,128)} %bitcast.44), calls=%async_computation.1 | async-start | bytes 4096 | tf_op jit(solution)/shard_map/all_to_all | solution.py:118
  13.0 5.3 %copy-start.2 = (bf16[8,128,2048]{2,1,0:T(8,128)(2,1)S(1)}, bf16[8,128,2048]{2,1,0:T(8,128)(2,1)}, u32[]{:S(2)}) copy-start(bf16[8,128,2048]{2,1,0:T(8,128)(2,1)} %param.17) | copy-start | bytes 12582916
  18.4 3.0 %copy-start.4 = (bf16[512,2048]{1,0:T(8,128)(2,1)S(1)}, bf16[512,2048]{1,0:T(8,128)(2,1)}, u32[]{:S(2)}) copy-start(bf16[512,2048]{1,0:T(8,128)(2,1)} %param.16) | copy-start | bytes 6291460
  18.4 3.0 %copy-start.10 = (bf16[2048,512]{1,0:T(8,128)(2,1)S(1)}, bf16[2048,512]{1,0:T(8,128)(2,1)}, u32[]{:S(2)}) copy-start(bf16[2048,512]{1,0:T(8,128)(2,1)} %param.27) | copy-start | bytes 6291460
  18.4 3.0 %copy-start.13 = (f32[2048]{0:T(1024)S(1)}, f32[2048]{0:T(1024)}, u32[]{:S(2)}) copy-start(f32[2048]{0:T(1024)} %param.25) | copy-start | bytes 24580
  33.0 63.8 %all-to-all-start = ((bf16[4,16,64,512]{3,2,1,0:T(8,128)(2,1)}), bf16[4,16,64,512]{3,2,1,0:T(8,128)(2,1)}, u32[]{:S(2)}, u32[]{:S(2)}) async-start(bf16[4,16,64,512]{3,2,1,0:T(8,128)(2,1)} %bitcast.116), calls=%async_computation | async-start | bytes 8388608 | tf_op jit(solution)/shard_map/all_to_all | solution.py:140
  38.0 5.4 %copy-start.3 = (bf16[1024,2048]{1,0:T(8,128)(2,1)S(1)}, bf16[1024,2048]{1,0:T(8,128)(2,1)}, u32[]{:S(2)}) copy-start(bf16[1024,2048]{1,0:T(8,128)(2,1)} %fusion.1) | copy-start | bytes 12582916
  38.0 5.4 %copy-start.11 = (bf16[2048,512]{1,0:T(8,128)(2,1)S(1)}, bf16[2048,512]{1,0:T(8,128)(2,1)}, u32[]{:S(2)}) copy-start(bf16[2048,512]{1,0:T(8,128)(2,1)} %param.28) | copy-start | bytes 6291460
  112.4 8.1 %all-to-all-start.2 = ((f32[4,1,2048]{2,1,0:T(1,128)}), f32[4,1,2048]{2,1,0:T(1,128)S(1)}, u32[]{:S(2)}, u32[]{:S(2)}) async-start(f32[4,1,2048]{2,1,0:T(1,128)} %reshape.590), calls=%async_computation.2 | async-start | bytes 65536 | tf_op jit(solution)/shard_map/all_to_all | solution.py:158
  120.5 27.5 %all-to-all-start.4 = ((f32[4,1,2048]{2,1,0:T(1,128)}), f32[4,1,2048]{2,1,0:T(1,128)S(1)}, u32[]{:S(2)}, u32[]{:S(2)}) async-start(f32[4,1,2048]{2,1,0:T(1,128)} %reshape.592), calls=%async_computation.4 | async-start | bytes 65536 | tf_op jit(solution)/shard_map/all_to_all | solution.py:165
  148.0 5.1 %copy-start.6 = (bf16[31,256]{1,0:T(8,128)(2,1)S(1)}, bf16[31,256]{1,0:T(8,128)(2,1)}, u32[]{:S(2)}) copy-start(bf16[31,256]{1,0:T(8,128)(2,1)} %param.22) | copy-start | bytes 47620
  148.0 5.2 %copy-start.14 = (f32[2048]{0:T(1024)S(1)}, f32[2048]{0:T(1024)}, u32[]{:S(2)}) copy-start(f32[2048]{0:T(1024)} %param.19) | copy-start | bytes 24580
  148.0 52.5 %all-to-all-start.3 = ((bf16[4,16,64,512]{3,2,1,0:T(8,128)(2,1)}), bf16[4,16,64,512]{3,2,1,0:T(8,128)(2,1)}, u32[]{:S(2)}, u32[]{:S(2)}) async-start(bf16[4,16,64,512]{3,2,1,0:T(8,128)(2,1)} %reshape_reshape.7), calls=%async_computation.3 | async-start | bytes 8388608 | tf_op jit(solution)/shard_map/all_to_all | solution.py:150
  153.1 105.1 %reduce-scatter.2.cloned.1.call-start = ((), (), s32[]{:S(2)}) async-start(), calls=%async_computation.6 | async-start | bytes 2621440 | tf_op jit(solution)/shard_map/reduce_scatter | solution.py:199
  153.1 2.9 %copy-start.5 = (bf16[512,2048]{1,0:T(8,128)(2,1)S(1)}, bf16[512,2048]{1,0:T(8,128)(2,1)}, u32[]{:S(2)}) copy-start(bf16[512,2048]{1,0:T(8,128)(2,1)} %param.16) | copy-start | bytes 6291460
  153.2 2.9 %copy-start.12 = (bf16[2048,256]{1,0:T(8,128)(2,1)S(1)}, bf16[2048,256]{1,0:T(8,128)(2,1)}, u32[]{:S(2)}) copy-start(bf16[2048,256]{1,0:T(8,128)(2,1)} %param.20) | copy-start | bytes 3145732
  156.0 10.8 %copy-start.9 = (f32[256]{0:T(256)S(1)}, f32[256]{0:T(256)}, u32[]{:S(2)}) copy-start(f32[256]{0:T(256)} %param.23) | copy-start | bytes 3076
  208.7 4.5 %copy-start.1 = (f32[512,2048]{1,0:T(8,128)S(1)}, f32[512,2048]{1,0:T(8,128)}, u32[]{:S(2)}) copy-start(f32[512,2048]{1,0:T(8,128)} %fusion.103) | copy-start | bytes 12582916
  208.8 4.5 %copy-start.7 = (f32[2048]{0:T(1024)S(1)}, f32[2048]{0:T(1024)}, u32[]{:S(2)}) copy-start(f32[2048]{0:T(1024)} %param.31) | copy-start | bytes 24580
Sparse Core Ops, SparseCore 0:
  216.2 42.0 reduce-scatter.1
where the time goes:
time: 270 us; the launch traced here: 265 us
  local copies, waits for them, and re-layouts  94.6 us (35%)
  waiting for transfers between devices  67.7 us (25%)
  matrix products  41 us (15%)
  starting transfers between devices  20.8 us (8%)
  other arithmetic  19.6 us (7%)
  between operations  13.8 us (5%)
  blocking collectives  7.64 us (3%)
    reduce_scatter x1, waiting for transfers between devices, local(): lax.psum_scatter((conv_term + blend_gain * attn_term).astype(jnp.bfloat16...  42.2 us
    all_to_all x1, waiting for transfers between devices, local(): lax.all_to_all(answer_out.reshape(owners, capacity, block_len, head_width...  25.4 us
    slice x2, local copies, waits for them, and re-layouts, passage_attention(): keys_values[:, :, span_width:]  23.5 us
    slice x1, local copies, waits for them, and re-layouts, passage_attention(): keys_values[:, :, :span_width]  11.9 us
    dot_general x1, matrix products, passage_attention(): jnp.einsum('ghqr,grhd->gqhd', weights, value_heads, preferred_element_typ...  10.1 us
    gather x1, local copies, waits for them, and re-layouts, local(): served = memory[asked.reshape(owners * capacity)]  8.88 us
    dot_general x1, matrix products, passage_attention(): jnp.einsum('gqhd,grhd->ghqr', query_heads, key_heads, preferred_element_t...  7.98 us
    psum x1, blocking collectives, local(): lax.psum((jnp.sum(conv_rows, axis=1), jnp.sum(conv_rows * conv_rows, axis...  7.64 us
  transfers between devices with their start and end apart: 6, of which 2 were waited for; matrix products, arithmetic and copies ran while one was open for 46% of the time, Pallas kernels for 0%

commit v1 on v0

v1 whole, which is shorter than its diff:
```python
import jax
import jax.numpy as jnp
from jax import lax
from jax.experimental import pallas as pl
from jax.experimental.pallas import tpu as pltpu
from jax.sharding import PartitionSpec as P

CA = 1024
HD = 256
SEQ_LEN = 128


EPS = 1e-06


def rms_rows(row_data, gain_vec):
    floats = row_data.astype(jnp.float32)
    inv_scale = lax.rsqrt(jnp.mean(floats * floats, axis=-1, keepdims=True) + EPS)
    return (floats * inv_scale * gain_vec).astype(jnp.bfloat16)


def depthwise(gated_rows, conv_taps):
    span_width = conv_taps.shape[0]
    half_span = (span_width - 1) // 2
    seq_length = gated_rows.shape[1]
    padded = jnp.pad(
        gated_rows.astype(jnp.float32), ((0, 0), (half_span, span_width - 1 - half_span), (0, 0))
    )
    running = jnp.zeros(gated_rows.shape, jnp.float32)
    for tap_index in range(span_width):
        running = running + padded[:, tap_index : tap_index + seq_length] * conv_taps[
            tap_index
        ].astype(jnp.float32)
    return running


NEVER = -1e30
BATCH = 4


def shifted(value, axis, step):
    size = lax.axis_size(axis)
    return lax.ppermute(value, axis, [(i, (i + step) % size) for i in range(size)])


def owner_attention(me, ids, query_list, keys, values, block_len, per_block, pass_rows):
    sources = len(query_list)
    rows, head_width = query_list[0].shape
    blocks = rows // block_len
    heads = head_width // HD
    held = keys.shape[0] // pass_rows
    slots = blocks * per_block + BATCH
    scale = HD ** (-0.5)
    pair = 128 // block_len

    def kernel(me_ref, ids_ref, *refs):
        query_refs = refs[:sources]
        key_ref, value_ref = refs[sources : sources + 2]
        out_refs = refs[sources + 2 : 2 * sources + 2]
        stat_refs = refs[2 * sources + 2 : 3 * sources + 2]
        list_block, list_pass, part_ref, top_ref, sum_ref = refs[3 * sources + 2 :]
        first = me_ref[0] * held
        lane = lax.broadcasted_iota(jnp.int32, (block_len, 128), 1)
        for source in range(sources):
            count = jnp.int32(0)
            starts = []
            for block in range(blocks):
                starts.append(count)
                for j in range(per_block):
                    where = ids_ref[source, block * per_block + j] - first
                    list_block[count] = jnp.int32(block)
                    list_pass[count] = jnp.clip(where, 0, held - 1)
                    mine = jnp.logical_and(where >= 0, where < held)
                    count = count + mine.astype(jnp.int32)
            starts.append(count)
            for u in range(BATCH):
                list_block[count + u] = jnp.int32(0)
                list_pass[count + u] = jnp.int32(0)
            trips = jnp.maximum((count + BATCH - 1) // BATCH, 1)
            query_ref = query_refs[source]

            def batch(i, carry):
                for u in range(BATCH):
                    slot = i * BATCH + u
                    block_at = pl.multiple_of(list_block[slot] * block_len, block_len)
                    pass_at = pl.multiple_of(list_pass[slot] * pass_rows, pass_rows)
                    for h in range(heads):
                        cols = slice(h * HD, (h + 1) * HD)
                        q = query_ref[pl.ds(block_at, block_len), cols]
                        k = key_ref[pl.ds(pass_at, pass_rows), cols]
                        v = value_ref[pl.ds(pass_at, pass_rows), cols]
                        scores = lax.dot_general(
                            q, k, (((1,), (1,)), ((), ())), preferred_element_type=jnp.float32
                        ) * scale
                        top = jnp.max(scores, axis=1, keepdims=True)
                        exponent = jnp.exp(scores - top)
                        total = jnp.sum(exponent, axis=1, keepdims=True)
                        out = jnp.dot(
                            exponent.astype(jnp.bfloat16), v, preferred_element_type=jnp.float32
                        )
                        part_ref[slot, :, cols] = out.astype(jnp.bfloat16)
                        top_ref[slot, h] = jnp.broadcast_to(top, (block_len, 128))
                        sum_ref[slot, h] = jnp.broadcast_to(total, (block_len, 128))
                return carry

            lax.fori_loop(0, trips, batch, 0)
            tiles = []
            for block in range(blocks):
                held_here = starts[block + 1] - starts[block]
                at = [
                    jnp.where(j < held_here, starts[block] + j, 0) for j in range(per_block)
                ]
                tile = jnp.zeros((block_len, 128), jnp.float32)
                for h in range(heads):
                    cols = slice(h * HD, (h + 1) * HD)
                    tops = [
                        jnp.where(j < held_here, top_ref[at[j], h], NEVER)
                        for j in range(per_block)
                    ]
                    best = tops[0]
                    for j in range(1, per_block):
                        best = jnp.maximum(best, tops[j])
                    total = jnp.zeros((block_len, 128), jnp.float32)
                    merged = jnp.zeros((block_len, HD), jnp.float32)
                    for j in range(per_block):
                        weight = jnp.where(j < held_here, jnp.exp(tops[j] - best), 0.0)
                        total = total + weight * sum_ref[at[j], h]
                        wide = jnp.concatenate([weight] * (HD // 128), axis=1)
                        merged = merged + wide * part_ref[at[j], :, cols].astype(jnp.float32)
                    out_refs[source][block * block_len : (block + 1) * block_len, cols] = (
                        merged.astype(jnp.bfloat16)
                    )
                    tile = jnp.where(lane == h, best, tile)
                    tile = jnp.where(lane == heads + h, total, tile)
                tiles.append(tile)
            for at_pair in range(0, blocks, pair):
                square = jnp.concatenate(tiles[at_pair : at_pair + pair], axis=0)
                stat_refs[source][:, at_pair * block_len : (at_pair + pair) * block_len] = (
                    square.T[:8]
                )

    whole = pl.BlockSpec(memory_space=pltpu.VMEM)
    scalar = pl.BlockSpec(memory_space=pltpu.SMEM)
    outs = pl.pallas_call(
        kernel,
        out_shape=[jax.ShapeDtypeStruct((rows, head_width), jnp.bfloat16)] * sources
        + [jax.ShapeDtypeStruct((8, rows), jnp.float32)] * sources,
        in_specs=[scalar, scalar] + [whole] * (sources + 2),
        out_specs=[whole] * (2 * sources),
        scratch_shapes=[
            pltpu.SMEM((slots,), jnp.int32),
            pltpu.SMEM((slots,), jnp.int32),
            pltpu.VMEM((slots, block_len, head_width), jnp.bfloat16),
            pltpu.VMEM((slots, heads, block_len, 128), jnp.float32),
            pltpu.VMEM((slots, heads, block_len, 128), jnp.float32),
        ],
        name="owner_attention",
    )(me, ids, *query_list, keys, values)
    return outs[:sources], outs[sources:]


def merge_owners(out_list, stat_list):
    sources = len(out_list)
    rows, head_width = out_list[0].shape
    heads = head_width // HD

    def kernel(*refs):
        out_refs = refs[:sources]
        stat_refs = refs[sources : 2 * sources]
        result_ref = refs[2 * sources]
        for at in range(0, rows, 128):
            stats = [ref[:, at : at + 128] for ref in stat_refs]
            best = [stats[0][h : h + 1] for h in range(heads)]
            for s in range(1, sources):
                best = [jnp.maximum(best[h], stats[s][h : h + 1]) for h in range(heads)]
            weights = [
                [jnp.exp(stats[s][h : h + 1] - best[h]) for h in range(heads)]
                for s in range(sources)
            ]
            for h in range(heads):
                total = weights[0][h] * stats[0][heads + h : heads + h + 1]
                for s in range(1, sources):
                    total = total + weights[s][h] * stats[s][heads + h : heads + h + 1]
                table = jnp.concatenate(
                    [weights[s][h] / total for s in range(sources)]
                    + [jnp.zeros((128 - sources, 128), jnp.float32)],
                    axis=0,
                ).T
                cols = slice(h * HD, (h + 1) * HD)
                merged = jnp.zeros((128, HD), jnp.float32)
                for s in range(sources):
                    merged = merged + table[:, s : s + 1] * out_refs[s][
                        at : at + 128, cols
                    ].astype(jnp.float32)
                result_ref[at : at + 128, cols] = merged.astype(jnp.bfloat16)

    whole = pl.BlockSpec(memory_space=pltpu.VMEM)
    return pl.pallas_call(
        kernel,
        out_shape=jax.ShapeDtypeStruct((rows, head_width), jnp.bfloat16),
        in_specs=[whole] * (2 * sources),
        out_specs=whole,
        name="merge_owners",
    )(*out_list, *stat_list)


def local(
    tokens,
    store,
    passage_ids,
    mix_gain,
    glu_value,
    glu_gate,
    conv_taps,
    channel_gain,
    mix_out,
    query_gain,
    passage_gain,
    query_proj,
    key_proj,
    value_proj,
    attn_out,
    blend_gain,
):
    owners = lax.axis_size("st")
    shards = lax.axis_size("tp")
    me = lax.axis_index("st").astype(jnp.int32)
    mine = lax.axis_index("tp")
    tok_rows, model_width = tokens.shape
    local_channels = glu_value.shape[1]
    head_width = query_proj.shape[1]
    block_count, per_block = passage_ids.shape
    block_len = tok_rows // block_count
    pass_local, pass_rows, _ = store.shape
    blocks_per_shard = block_count // shards
    chunks = CHUNKS if blocks_per_shard % CHUNKS == 0 else 1
    run = blocks_per_shard // chunks * block_len
    steps = range(1, owners)

    def cut(rows, c):
        return rows.reshape(shards, chunks, run, -1)[:, c].reshape(shards * run, -1)

    queries = jnp.dot(
        rms_rows(tokens, query_gain), query_proj, preferred_element_type=jnp.float32
    ).astype(jnp.bfloat16)
    id_list = [passage_ids] + [shifted(passage_ids, "st", k) for k in steps]
    all_ids = jnp.stack(id_list)
    query_chunks = []
    for c in range(chunks):
        own = cut(queries, c)
        query_chunks.append([own] + [shifted(own, "st", k) for k in steps])
    normed_store = rms_rows(store.reshape(pass_local * pass_rows, model_width), passage_gain)
    key_rows = jnp.dot(normed_store, key_proj, preferred_element_type=jnp.float32).astype(
        jnp.bfloat16
    )
    value_rows = jnp.dot(normed_store, value_proj, preferred_element_type=jnp.float32).astype(
        jnp.bfloat16
    )
    mix_input = rms_rows(tokens, mix_gain)
    value_part = jnp.dot(mix_input, glu_value, preferred_element_type=jnp.float32)
    gate_part = jnp.dot(mix_input, glu_gate, preferred_element_type=jnp.float32)
    gated_rows = (value_part * jax.nn.sigmoid(gate_part)).astype(jnp.bfloat16)
    conv_rows = depthwise(gated_rows.reshape(-1, SEQ_LEN, local_channels), conv_taps).reshape(
        tok_rows, local_channels
    )
    sums = jnp.stack([jnp.sum(conv_rows, axis=1), jnp.sum(conv_rows * conv_rows, axis=1)])
    channel_total = sums
    for k in range(1, shards):
        channel_total = channel_total + shifted(sums, "tp", k)
    answers = []
    for c in range(chunks):
        ids = all_ids.reshape(
            owners, shards, chunks, blocks_per_shard // chunks * per_block
        )[:, :, c].reshape(owners, -1)
        out_list, stat_list = owner_attention(
            me[None], ids, query_chunks[c], key_rows, value_rows, block_len, per_block, pass_rows
        )
        answers.append(
            (
                [out_list[0]] + [shifted(out_list[k], "st", -k) for k in steps],
                [stat_list[0]] + [shifted(stat_list[k], "st", -k) for k in steps],
            )
        )
    row_mean = channel_total[0] / CA
    row_var = channel_total[1] / CA - row_mean * row_mean
    activation = jax.nn.silu(
        (conv_rows - row_mean[:, None]) * lax.rsqrt(row_var + EPS)[:, None] * channel_gain
    ).astype(jnp.bfloat16)
    results = []
    for c in range(chunks):
        attended = merge_owners(*answers[c])
        conv_term = jnp.dot(cut(activation, c), mix_out, preferred_element_type=jnp.float32)
        attn_term = jnp.dot(attended, attn_out, preferred_element_type=jnp.float32)
        partial = (
            (conv_term + blend_gain * attn_term).astype(jnp.bfloat16).reshape(shards, run, -1)
        )
        order = sorted(range(1, shards), key=lambda k: -min(k, shards - k))
        pieces = [
            shifted(
                lax.dynamic_index_in_dim(partial, (mine + k) % shards, 0, keepdims=False),
                "tp",
                k,
            )
            for k in order
        ]
        total = lax.dynamic_index_in_dim(partial, mine, 0, keepdims=False).astype(jnp.float32)
        for piece in pieces:
            total = total + piece.astype(jnp.float32)
        results.append(total.astype(jnp.bfloat16))
    return jnp.concatenate(results, axis=0)


CHUNKS = 2


def solution(mesh):
    in_specs = (
        P(("grp", "st"), None),
        P(("grp", "st"), None, None),
        P(("grp", "st"), None),
        P(),
        P(None, "tp"),
        P(None, "tp"),
        P(None, "tp"),
        P("tp"),
        P("tp", None),
        P(),
        P(),
        P(None, "tp"),
        P(None, "tp"),
        P(None, "tp"),
        P("tp", None),
        P(),
    )
    out_specs = P(("grp", "st", "tp"), None)
    return jax.shard_map(local, mesh=mesh, in_specs=in_specs, out_specs=out_specs, check_vma=False)
```

time: 270 us -> 166 us (0.61); the launches traced: 265 us -> 167 us
  local copies, waits for them, and re-layouts: 94.6 us -> 5.72 us
  Pallas kernels: 0 us -> 52.6 us
  waiting for transfers between devices: 67.7 us -> 36.1 us
  matrix products: 41 us -> 22.5 us
  starting transfers between devices: 20.8 us -> 36.6 us
  between operations: 13.8 us -> 0.4 us
  blocking collectives: 7.64 us -> 0 us
  other arithmetic: 19.6 us -> 13 us
    pallas_call x0 -> x4, Pallas kernels: none -> 52.6 us  [the longest x2 47.5 us: owner_attention(): pl.pallas_call(kernel, out_shape=[jax.ShapeDtypeStruct((rows, head_width)...]
    reduce_scatter x1 -> x0, waiting for transfers between devices: 42.2 us -> none  [local(): lax.psum_scatter((conv_term + blend_gain * attn_term).astype(jnp.bfloat16...]
    ppermute x0 -> x30, starting transfers between devices: none -> 36.6 us  [shifted(): lax.ppermute(value, axis, [(i, (i + step) % size) for i in range(size)])]
    ppermute x0 -> x30, waiting for transfers between devices: none -> 36.1 us  [shifted(): lax.ppermute(value, axis, [(i, (i + step) % size) for i in range(size)])]
    slice x3, local copies, waits for them, and re-layouts: 35.3 us -> 1.48 us  [the longest x2 1.42 us: cut(): return rows.reshape(shards, chunks, run, -1)[:, c].reshape(shards * run, -1)]
    all_to_all x5 -> x0, waiting for transfers between devices: 25.5 us -> none  [the longest x1 25.4 us: local(): lax.all_to_all(answer_out.reshape(owners, capacity, block_len, head_width...]
    dot_general x4 -> x2, matrix products: 25.6 us -> 4.48 us  [local(): jnp.dot(cut(activation, c), mix_out, preferred_element_type=jnp.float32)]
    all_to_all x5 -> x0, starting transfers between devices: 20.8 us -> none  [the longest x1 5.09 us: local(): lax.all_to_all(answer_out.reshape(owners, capacity, block_len, head_width...]
  transfers between devices with their start and end apart: 6 -> 30, of which waited for: 2 -> 8; matrix products, arithmetic and copies ran while one was open for 46% -> 23% of each run, Pallas kernels for 0% -> 32%
where the time goes in v1:
time: 166 us; the launch traced here: 167 us
  Pallas kernels  52.6 us (32%)
  starting transfers between devices  36.6 us (22%)
  waiting for transfers between devices  36.1 us (22%)
  matrix products  22.5 us (14%)
  other arithmetic  13 us (8%)
  local copies, waits for them, and re-layouts  5.72 us (3%)
    pallas_call x2, Pallas kernels, owner_attention(): pl.pallas_call(kernel, out_shape=[jax.ShapeDtypeStruct((rows, head_width)...  47.5 us
    ppermute x30, starting transfers between devices, shifted(): lax.ppermute(value, axis, [(i, (i + step) % size) for i in range(size)])  36.6 us
    ppermute x30, waiting for transfers between devices, shifted(): lax.ppermute(value, axis, [(i, (i + step) % size) for i in range(size)])  36.1 us
    reduce_sum x2, other arithmetic, rms_rows(): jnp.mean(floats * floats, axis=-1, keepdims=True) + EPS  5.3 us
    pallas_call x2, Pallas kernels, merge_owners(): pl.pallas_call(kernel, out_shape=jax.ShapeDtypeStruct((rows, head_width),...  5.11 us
    dot_general x2, matrix products, local(): attn_term = jnp.dot(attended, attn_out, preferred_element_type=jnp.float32)  4.82 us
    dot_general x2, matrix products, local(): jnp.dot(cut(activation, c), mix_out, preferred_element_type=jnp.float32)  4.48 us
    dot_general x1, matrix products, local(): jnp.dot(normed_store, key_proj, preferred_element_type=jnp.float32)  3.35 us
  transfers between devices with their start and end apart: 30, of which 8 were waited for; matrix products, arithmetic and copies ran while one was open for 23% of the time, Pallas kernels for 32%

profile of v1, /device:TPU:9, one launch (start us, length us, event | category | flops | bytes accessed | tf_op | source)
XLA Modules:
  0.0 166.9 jit_solution(2761087405386787829)
XLA Ops:
  0.0 0.9 copy.17
  0.9 1.8 %collective-permute-start.3 = (s32[8,4]{1,0:T(8,128)S(1)}, s32[8,4]{1,0:T(8,128)S(1)}, u32[]{:S(2)}, u32[]{:S(2)}) collective-permute-start(s32[8,4]{1,0:T(8,128)S(1)} %copy.17), channel_id=1, source_target_pairs={{0,4},{4,8},{8,12},{12,0},{1,5},{5,9},{9,13},{13,1},{2,6},{6,10},{... | collective-permute-start | bytes 392 | tf_op jit(solution)/shard_map/ppermute | solution.py:43
  3.1 2.1 %fusion.6 = f32[512]{0:T(512)S(1)} fusion(bf16[512,2048]{1,0:T(8,128)(2,1)} %param.16), kind=kLoop, calls=%fused_computation.10 | loop fusion | flops 3145216 | bytes 2099200 | tf_op jit(solution)/shard_map/reduce_sum | solution.py:18
  5.2 2.9 %fusion.15 = bf16[512,512]{1,0:T(8,128)(2,1)S(1)} fusion(bf16[2048,512]{1,0:T(8,128)(2,1)} %param.27, bf16[512,2048]{1,0:T(8,128)(2,1)S(1)} %copy-done.3, f32[2048]{0:T(1024)S(1)} %copy-done.19, f32[512]{0:T(512)S(1)} %add_rsqrt_fusion.1), kind=kOutput, calls=%fused_computation.52 | convolution fusion | flops 1078198272 | bytes 4728832 | tf_op jit(solution)/shard_map/dot_general | solution.py:243
  8.1 0.7 fusion.94
  8.9 1.6 collective-permute-start.6
  10.5 1.2 collective-permute-start.7
  11.8 3.2 %multiply_reduce_fusion = f32[8,128]{1,0:T(8,128)S(1)} fusion(bf16[8,128,2048]{2,1,0:T(8,128)(2,1)} %param.17), kind=kLoop, calls=%fused_computation.3 | loop fusion | flops 6290432 | bytes 4198400 | tf_op jit(solution)/shard_map/reduce_sum | solution.py:18
  15.3 1.0 fusion.1
  16.8 3.3 %convolution_convert_fusion.refs_5_ = bf16[1024,512]{1,0:T(8,128)(2,1)} fusion(bf16[1024,2048]{1,0:T(8,128)(2,1)S(1)} %fusion.1, bf16[2048,512]{1,0:T(8,128)(2,1)S(1)} %copy-done.16), kind=kOutput, calls=%fused_computation.20 | convolution fusion | flops 2148007936 | bytes 7340032 | tf_op jit(solution)/shard_map/dot_general | solution.py:256
  20.2 3.4 %convolution_convert_fusion.1.refs_4_ = bf16[1024,512]{1,0:T(8,128)(2,1)} fusion(bf16[1024,2048]{1,0:T(8,128)(2,1)S(1)} %fusion.1, bf16[2048,512]{1,0:T(8,128)(2,1)S(1)} %copy-done.17), kind=kOutput, calls=%fused_computation.21 | convolution fusion | flops 2148007936 | bytes 7340032 | tf_op jit(solution)/shard_map/dot_general | solution.py:253
  23.5 2.8 %fusion.20 = f32[512,256]{1,0:T(8,128)S(1)} fusion(bf16[2048,256]{1,0:T(8,128)(2,1)} %param.21, bf16[512,2048]{1,0:T(8,128)(2,1)} %param.16, f32[2048]{0:T(1024)S(1)} %copy-done.20, f32[512]{0:T(512)S(1)} %add_rsqrt_fusion.1), kind=kOutput, calls=%fused_computation.57 | convolution fusion | flops 541458432 | bytes 3680256 | tf_op jit(solution)/shard_map/dot_general | solution.py:261
  26.4 0.8 bitcast_convert_fusion
  27.1 2.9 %fusion.92 = (f32[4,128]{1,0:T(4,128)S(1)}, f32[4,128]{1,0:T(4,128)S(1)}, f32[4,128,256]{2,1,0:T(8,128)}) fusion(f32[256]{0:T(256)S(1)} %bitcast.142, f32[256]{0:T(256)S(1)} %bitcast.143, f32[256]{0:T(256)S(1)} %bitcast.114, f32[256]{0:T(256)S(1)} %bitcast.115, f32[256]{0:T(256)S(1)} %bitcast.116, f32[256]{0:T(256)S(1)} %bitcast.117, f32[256]{0:T(256)S(1)} %bitcast.118, ...), kind=kLoop, calls=%fused_computation.179 | loop fusion | flops 8387584 | bytes 1084416 | tf_op jit(solution)/shard_map/reduce_sum | solution.py:266
  30.1 1.4 collective-permute-start
  31.5 1.1 collective-permute-start.1
  32.6 1.4 collective-permute-start.2
  35.4 1.7 %collective-permute-start.18 = (bf16[256,512]{1,0:T(8,128)(2,1)S(1)}, bf16[256,512]{1,0:T(8,128)(2,1)}, u32[]{:S(2)}, u32[]{:S(2)}) collective-permute-start(bf16[256,512]{1,0:T(8,128)(2,1)S(1)} %bitcast.101), channel_id=1, source_target_pairs={{0,4},{4,8},{8,12},{12,0},{1,5},{5,9},{9,13},{13,1},{2,6},{6,10},{... | collective-permute-start | bytes 786440 | tf_op jit(solution)/shard_map/ppermute | solution.py:43
  37.6 1.4 multiply_convert_fusion
  38.9 0.7 fusion.95
  39.9 4.4 %collective-permute-done.8.refs_3_ = bf16[256,512]{1,0:T(8,128)(2,1)} collective-permute-done((bf16[256,512]{1,0:T(8,128)(2,1)}, bf16[256,512]{1,0:T(8,128)(2,1)}, u32[]{:S(2)}, u32[]{:S(2)}) %collective-permute-start.8) | collective-permute-done | bytes 262176 | tf_op jit(solution)/shard_map/ppermute | solution.py:43
  44.3 26.8 %owner_attention.2 = (bf16[256,512]{1,0:T(8,128)(2,1)}, bf16[256,512]{1,0:T(8,128)(2,1)}, bf16[256,512]{1,0:T(8,128)(2,1)}, bf16[256,512]{1,0:T(8,128)(2,1)}, f3...) custom-call(s32[1]{0:T(128)} %bitcast.37.me_ref, s32[4,16]{1,0:T(4,128)} %reshape_squeeze.19.ids_ref, ...), custom_call_target="tpu_custom_call" | custom-call | tf_op jit(solution)/shard_map/owner_attention/pallas_call | solution.py:144
  71.2 2.7 %fusion.96 = f32[256,2048]{1,0:T(8,128)} fusion(bf16[256,256]{1,0:T(8,128)(2,1)} %bitcast.107, bf16[256,2048]{1,0:T(8,128)(2,1)S(1)} %copy-done.2), kind=kOutput, calls=%fused_computation.183 | convolution fusion | flops 268435456 | bytes 3276800 | tf_op jit(solution)/shard_map/dot_general | solution.py:292
  73.8 1.7 %collective-permute-start.11 = (bf16[256,512]{1,0:T(8,128)(2,1)}, bf16[256,512]{1,0:T(8,128)(2,1)}, u32[]{:S(2)}, u32[]{:S(2)}) collective-permute-start(bf16[256,512]{1,0:T(8,128)(2,1)} %get-tuple-element.24), channel_id=1, source_target_pairs={{0,4},{4,8},{8,12},{12,0},{1,5},{5,9},{9,13},{13,1},{2,6},{6,10},{... | collective-permute-start | bytes 786440 | tf_op jit(solution)/shard_map/ppermute | solution.py:43
  76.0 1.4 collective-permute-start.13
  77.4 2.0 %collective-permute-start.14 = (f32[8,256]{1,0:T(8,128)S(1)}, f32[8,256]{1,0:T(8,128)S(1)}, u32[]{:S(2)}, u32[]{:S(2)}) collective-permute-start(f32[8,256]{1,0:T(8,128)S(1)} %copy-done.22), channel_id=1, source_target_pairs={{0,4},{4,8},{8,12},{12,0},{1,5},{5,9},{9,13},{13,1},{2,6},{6,10},{... | collective-permute-start | bytes 24584 | tf_op jit(solution)/shard_map/ppermute | solution.py:43
  79.4 1.8 %fusion.97 = f32[256,2048]{1,0:T(8,128)} fusion(bf16[256,256]{1,0:T(8,128)(2,1)S(1)} %bitcast.106, bf16[256,2048]{1,0:T(8,128)(2,1)S(1)} %copy-done.2), kind=kOutput, calls=%fused_computation.184 | convolution fusion | flops 268435456 | bytes 3276800 | tf_op jit(solution)/shard_map/dot_general | solution.py:292
  81.2 20.7 %owner_attention.3 = (bf16[256,512]{1,0:T(8,128)(2,1)}, bf16[256,512]{1,0:T(8,128)(2,1)}, bf16[256,512]{1,0:T(8,128)(2,1)}, bf16[256,512]{1,0:T(8,128)(2,1)}, f3...) custom-call(s32[1]{0:T(128)} %bitcast.37.me_ref, s32[4,16]{1,0:T(4,128)} %reshape_squeeze.22.ids_ref, ...), custom_call_target="tpu_custom_call" | custom-call | tf_op jit(solution)/shard_map/owner_attention/pallas_call | solution.py:144
  102.1 1.7 %collective-permute-start.23 = (bf16[256,512]{1,0:T(8,128)(2,1)}, bf16[256,512]{1,0:T(8,128)(2,1)}, u32[]{:S(2)}, u32[]{:S(2)}) collective-permute-start(bf16[256,512]{1,0:T(8,128)(2,1)} %get-tuple-element.32), channel_id=1, source_target_pairs={{0,4},{4,8},{8,12},{12,0},{1,5},{5,9},{9,13},{13,1},{2,6},{6,10},{... | collective-permute-start | bytes 786440 | tf_op jit(solution)/shard_map/ppermute | solution.py:43
  104.2 1.4 collective-permute-start.25
  105.6 2.6 %merge_owners.2 = bf16[256,512]{1,0:T(8,128)(2,1)} custom-call(bf16[256,512]{1,0:T(8,128)(2,1)} %get-tuple-element.21.refs_0_, bf16[256,512]{1,0:T(8,128)(2,1)} %collective-permute-done.9.refs_1_, bf16[256,512]{1,0:T(8,128)(2,1)} %collective-permute-done.10.refs_2_, bf16[256,512]{1,0:T(8,128)(2,1)} %collective-permute-done.11.refs_3_, ...), custom_call_target="tpu_custom_call" | custom-call | tf_op jit(solution)/shard_map/merge_owners/pallas_call | solution.py:198
  108.2 2.4 %fusion.9 = bf16[256,2048]{1,0:T(8,128)(2,1)S(1)} fusion(f32[256,2048]{1,0:T(8,128)} %fusion.96, bf16[256,512]{1,0:T(8,128)(2,1)} %merge_owners.2, bf16[512,2048]{1,0:T(8,128)(2,1)S(1)} %copy-done, f32[2048]{0:T(1024)S(1)} %copy-done.7), kind=kOutput, calls=%fused_computation.15 | convolution fusion | flops 538443776 | bytes 5513216 | tf_op jit(solution)/shard_map/dot_general | solution.py:293
  110.6 5.9 %collective-permute-done.24.refs_5_ = f32[8,256]{1,0:T(8,128)S(1)} collective-permute-done((f32[8,256]{1,0:T(8,128)}, f32[8,256]{1,0:T(8,128)S(1)}, u32[]{:S(2)}, u32[]{:S(2)}) %collective-permute-start.24) | collective-permute-done | bytes 8224 | tf_op jit(solution)/shard_map/ppermute | solution.py:43
  116.5 0.9 dynamic-slice_bitcast_fusion.5
  117.7 2.0 %collective-permute-start.16 = (bf16[64,2048]{1,0:T(8,128)(2,1)}, bf16[64,2048]{1,0:T(8,128)(2,1)}, u32[]{:S(2)}, u32[]{:S(2)}) collective-permute-start(bf16[64,2048]{1,0:T(8,128)(2,1)} %get-tuple-element.46), channel_id=1, source_target_pairs={{0,1},{1,2},{2,3},{3,0},{4,5},{5,6},{6,7},{7,4},{8,9},{9,10},{10,1... | collective-permute-start | bytes 786440 | tf_op jit(solution)/shard_map/ppermute | solution.py:43
  119.8 2.5 %merge_owners.3 = bf16[256,512]{1,0:T(8,128)(2,1)} custom-call(bf16[256,512]{1,0:T(8,128)(2,1)} %get-tuple-element.29.refs_0_, bf16[256,512]{1,0:T(8,128)(2,1)} %collective-permute-done.21.refs_1_, bf16[256,512]{1,0:T(8,128)(2,1)} %collective-permute-done.22.refs_2_, bf16[256,512]{1,0:T(8,128)(2,1)} %collective-permute-done.23.refs_3_, ...), custom_call_target="tpu_custom_call" | custom-call | tf_op jit(solution)/shard_map/merge_owners/pallas_call | solution.py:198
  122.3 2.4 %fusion.10 = bf16[256,2048]{1,0:T(8,128)(2,1)S(1)} fusion(f32[256,2048]{1,0:T(8,128)} %fusion.97, bf16[256,512]{1,0:T(8,128)(2,1)} %merge_owners.3, bf16[512,2048]{1,0:T(8,128)(2,1)S(1)} %copy-done, f32[2048]{0:T(1024)S(1)} %copy-done.7), kind=kOutput, calls=%fused_computation.16 | convolution fusion | flops 538443776 | bytes 5513216 | tf_op jit(solution)/shard_map/dot_general | solution.py:293
  124.8 1.6 collective-permute-start.27
  126.4 1.9 %collective-permute-start.28 = (bf16[64,2048]{1,0:T(8,128)(2,1)S(1)}, bf16[64,2048]{1,0:T(8,128)(2,1)S(1)}, u32[]{:S(2)}, u32[]{:S(2)}) collective-permute-start(bf16[64,2048]{1,0:T(8,128)(2,1)S(1)} %get-tuple-element.49), channel_id=1, source_target_pairs={{0,1},{1,2},{2,3},{3,0},{4,5},{5,6},{6,7},{7,4},{8,9},{9,10},{10,1... | collective-permute-start | bytes 786440 | tf_op jit(solution)/shard_map/ppermute | solution.py:43
  128.3 0.7 collective-permute-done.15
  129.0 10.6 %collective-permute-start.29 = (bf16[64,2048]{1,0:T(8,128)(2,1)S(1)}, bf16[64,2048]{1,0:T(8,128)(2,1)S(1)}, u32[]{:S(2)}, u32[]{:S(2)}) collective-permute-start(bf16[64,2048]{1,0:T(8,128)(2,1)S(1)} %get-tuple-element.48), channel_id=1, source_target_pairs={{0,3},{1,0},{2,1},{3,2},{4,7},{5,4},{6,5},{7,6},{8,11},{9,8},{10,9... | collective-permute-start | bytes 786440 | tf_op jit(solution)/shard_map/ppermute | solution.py:43
  139.6 6.3 %collective-permute-done.16 = bf16[64,2048]{1,0:T(8,128)(2,1)} collective-permute-done((bf16[64,2048]{1,0:T(8,128)(2,1)}, bf16[64,2048]{1,0:T(8,128)(2,1)}, u32[]{:S(2)}, u32[]{:S(2)}) %collective-permute-start.16) | collective-permute-done | bytes 262176 | tf_op jit(solution)/shard_map/ppermute | solution.py:43
  145.9 8.9 %collective-permute-done.17 = bf16[64,2048]{1,0:T(8,128)(2,1)} collective-permute-done((bf16[64,2048]{1,0:T(8,128)(2,1)S(1)}, bf16[64,2048]{1,0:T(8,128)(2,1)}, u32[]{:S(2)}, u32[]{:S(2)}) %collective-permute-start.17) | collective-permute-done | bytes 262176 | tf_op jit(solution)/shard_map/ppermute | solution.py:43
  154.7 1.2 fusion.89
  156.0 1.0 collective-permute-done.27
  157.0 5.6 %collective-permute-done.28 = bf16[64,2048]{1,0:T(8,128)(2,1)S(1)} collective-permute-done((bf16[64,2048]{1,0:T(8,128)(2,1)S(1)}, bf16[64,2048]{1,0:T(8,128)(2,1)S(1)}, u32[]{:S(2)}, u32[]{:S(2)}) %collective-permute-start.28) | collective-permute-done | bytes 262176 | tf_op jit(solution)/shard_map/ppermute | solution.py:43
  162.6 3.2 %collective-permute-done.29 = bf16[64,2048]{1,0:T(8,128)(2,1)S(1)} collective-permute-done((bf16[64,2048]{1,0:T(8,128)(2,1)S(1)}, bf16[64,2048]{1,0:T(8,128)(2,1)S(1)}, u32[]{:S(2)}, u32[]{:S(2)}) %collective-permute-start.29) | collective-permute-done | bytes 262176 | tf_op jit(solution)/shard_map/ppermute | solution.py:43
  166.0 0.8 pad_maximum_fusion
  (98 shorter events, 4.9 us)
Async XLA Ops:
  0.0 108.1 %copy-start = (bf16[512,2048]{1,0:T(8,128)(2,1)S(1)}, bf16[512,2048]{1,0:T(8,128)(2,1)}, u32[]{:S(2)}) copy-start(bf16[512,2048]{1,0:T(8,128)(2,1)} %param.30) | copy-start | bytes 6291460
  0.0 5.2 %copy-start.19 = (f32[2048]{0:T(1024)S(1)}, f32[2048]{0:T(1024)}, u32[]{:S(2)}) copy-start(f32[2048]{0:T(1024)} %param.25) | copy-start | bytes 24580
  0.9 4.3 %copy-start.3 = (bf16[512,2048]{1,0:T(8,128)(2,1)S(1)}, bf16[512,2048]{1,0:T(8,128)(2,1)}, u32[]{:S(2)}) copy-start(bf16[512,2048]{1,0:T(8,128)(2,1)} %param.16) | copy-start | bytes 6291460
  0.9 29.2 %collective-permute-start.3 = (s32[8,4]{1,0:T(8,128)S(1)}, s32[8,4]{1,0:T(8,128)S(1)}, u32[]{:S(2)}, u32[]{:S(2)}) collective-permute-start(s32[8,4]{1,0:T(8,128)S(1)} %copy.17), channel_id=1, source_target_pairs={{0,4},{4,8},{8,12},{12,0},{1,5},{5,9},{9,13},{13,1},{2,6},{6,10},{... | collective-permute-start | bytes 392 | tf_op jit(solution)/shard_map/ppermute | solution.py:43
  2.7 28.8 %collective-permute-start.4 = (s32[8,4]{1,0:T(8,128)S(1)}, s32[8,4]{1,0:T(8,128)S(1)}, u32[]{:S(2)}, u32[]{:S(2)}) collective-permute-start(s32[8,4]{1,0:T(8,128)S(1)} %copy.17), channel_id=1, source_target_pairs={{0,8},{4,12},{8,0},{12,4},{1,9},{5,13},{9,1},{13,5},{2,10},{6,14},... | collective-permute-start | bytes 392 | tf_op jit(solution)/shard_map/ppermute | solution.py:43
  3.0 29.6 %collective-permute-start.5 = (s32[8,4]{1,0:T(8,128)S(1)}, s32[8,4]{1,0:T(8,128)S(1)}, u32[]{:S(2)}, u32[]{:S(2)}) collective-permute-start(s32[8,4]{1,0:T(8,128)S(1)} %copy.17), channel_id=1, source_target_pairs={{0,12},{4,0},{8,4},{12,8},{1,13},{5,1},{9,5},{13,9},{2,14},{6,2},{... | collective-permute-start | bytes 392 | tf_op jit(solution)/shard_map/ppermute | solution.py:43
  5.2 6.5 %copy-start.6 = (bf16[31,256]{1,0:T(8,128)(2,1)S(1)}, bf16[31,256]{1,0:T(8,128)(2,1)}, u32[]{:S(2)}) copy-start(bf16[31,256]{1,0:T(8,128)(2,1)} %param.22) | copy-start | bytes 47620
  8.9 30.7 %copy-start.5 = (bf16[4,1,64,512]{3,2,1,0:T(8,128)(2,1)}, bf16[4,1,64,512]{3,2,1,0:T(8,128)(2,1)S(1)}, u32[]{:S(2)}) copy-start(bf16[4,1,64,512]{3,2,1,0:T(8,128)(2,1)S(1)} %get-tuple-element.51) | copy-start | bytes 786436
  8.9 30.7 %collective-permute-start.6 = (bf16[256,512]{1,0:T(8,128)(2,1)}, bf16[256,512]{1,0:T(8,128)(2,1)}, u32[]{:S(2)}, u32[]{:S(2)}) collective-permute-start(bf16[256,512]{1,0:T(8,128)(2,1)} %bitcast.43.refs_0_), channel_id=1, source_target_pairs={{0,4},{4,8},{8,12},{12,0},{1,5},{5,9},{9,13},{13,1},{2,6},{6,10},{... | collective-permute-start | bytes 786440 | tf_op jit(solution)/shard_map/ppermute | solution.py:43
  10.5 29.4 %collective-permute-start.7 = (bf16[256,512]{1,0:T(8,128)(2,1)}, bf16[256,512]{1,0:T(8,128)(2,1)}, u32[]{:S(2)}, u32[]{:S(2)}) collective-permute-start(bf16[256,512]{1,0:T(8,128)(2,1)} %bitcast.43.refs_0_), channel_id=1, source_target_pairs={{0,8},{4,12},{8,0},{12,4},{1,9},{5,13},{9,1},{13,5},{2,10},{6,14},... | collective-permute-start | bytes 786440 | tf_op jit(solution)/shard_map/ppermute | solution.py:43
  11.8 3.5 %copy-start.1 = (bf16[8,128,2048]{2,1,0:T(8,128)(2,1)S(1)}, bf16[8,128,2048]{2,1,0:T(8,128)(2,1)}, u32[]{:S(2)}) copy-start(bf16[8,128,2048]{2,1,0:T(8,128)(2,1)} %param.17) | copy-start | bytes 12582916
  11.8 3.4 %copy-start.8 = (f32[2048]{0:T(1024)S(1)}, f32[2048]{0:T(1024)}, u32[]{:S(2)}) copy-start(f32[2048]{0:T(1024)} %param.26) | copy-start | bytes 24580
  16.8 3.3 %copy-start.17 = (bf16[2048,512]{1,0:T(8,128)(2,1)S(1)}, bf16[2048,512]{1,0:T(8,128)(2,1)}, u32[]{:S(2)}) copy-start(bf16[2048,512]{1,0:T(8,128)(2,1)} %param.28) | copy-start | bytes 6291460
  20.2 3.4 %copy-start.20 = (f32[2048]{0:T(1024)S(1)}, f32[2048]{0:T(1024)}, u32[]{:S(2)}) copy-start(f32[2048]{0:T(1024)} %param.19) | copy-start | bytes 24580
  26.4 11.2 %copy-start.15 = (f32[256]{0:T(256)S(1)}, f32[256]{0:T(256)}, u32[]{:S(2)}) copy-start(f32[256]{0:T(256)} %param.23) | copy-start | bytes 3076
  30.1 5.2 %collective-permute-start = (f32[2,512]{1,0:T(2,128)S(1)}, f32[2,512]{1,0:T(2,128)S(1)}, u32[]{:S(2)}, u32[]{:S(2)}) collective-permute-start(f32[2,512]{1,0:T(2,128)S(1)} %pad_maximum_fusion.1), channel_id=1, source_target_pairs={{0,1},{1,2},{2,3},{3,0},{4,5},{5,6},{6,7},{7,4},{8,9},{9,10},{10,1... | collective-permute-start | bytes 12296 | tf_op jit(solution)/shard_map/ppermute | solution.py:43
  31.5 3.9 %collective-permute-start.1 = (f32[2,512]{1,0:T(2,128)S(1)}, f32[2,512]{1,0:T(2,128)S(1)}, u32[]{:S(2)}, u32[]{:S(2)}) collective-permute-start(f32[2,512]{1,0:T(2,128)S(1)} %pad_maximum_fusion.1), channel_id=1, source_target_pairs={{0,2},{1,3},{2,0},{3,1},{4,6},{5,7},{6,4},{7,5},{8,10},{9,11},{10,... | collective-permute-start | bytes 12296 | tf_op jit(solution)/shard_map/ppermute | solution.py:43
  32.6 4.5 %collective-permute-start.2 = (f32[2,512]{1,0:T(2,128)S(1)}, f32[2,512]{1,0:T(2,128)S(1)}, u32[]{:S(2)}, u32[]{:S(2)}) collective-permute-start(f32[2,512]{1,0:T(2,128)S(1)} %pad_maximum_fusion.1), channel_id=1, source_target_pairs={{0,3},{1,0},{2,1},{3,2},{4,7},{5,4},{6,5},{7,6},{8,11},{9,8},{10,9... | collective-permute-start | bytes 12296 | tf_op jit(solution)/shard_map/ppermute | solution.py:43
  35.4 8.9 %collective-permute-start.8 = (bf16[256,512]{1,0:T(8,128)(2,1)}, bf16[256,512]{1,0:T(8,128)(2,1)}, u32[]{:S(2)}, u32[]{:S(2)}) collective-permute-start(bf16[256,512]{1,0:T(8,128)(2,1)} %bitcast.43.refs_0_), channel_id=1, source_target_pairs={{0,12},{4,0},{8,4},{12,8},{1,13},{5,1},{9,5},{13,9},{2,14},{6,2},{... | collective-permute-start | bytes 786440 | tf_op jit(solution)/shard_map/ppermute | solution.py:43
  35.4 38.5 %collective-permute-start.18 = (bf16[256,512]{1,0:T(8,128)(2,1)S(1)}, bf16[256,512]{1,0:T(8,128)(2,1)}, u32[]{:S(2)}, u32[]{:S(2)}) collective-permute-start(bf16[256,512]{1,0:T(8,128)(2,1)S(1)} %bitcast.101), channel_id=1, source_target_pairs={{0,4},{4,8},{8,12},{12,0},{1,5},{5,9},{9,13},{13,1},{2,6},{6,10},{... | collective-permute-start | bytes 786440 | tf_op jit(solution)/shard_map/ppermute | solution.py:43
  37.1 38.4 %collective-permute-start.19 = (bf16[256,512]{1,0:T(8,128)(2,1)S(1)}, bf16[256,512]{1,0:T(8,128)(2,1)}, u32[]{:S(2)}, u32[]{:S(2)}) collective-permute-start(bf16[256,512]{1,0:T(8,128)(2,1)S(1)} %bitcast.102), channel_id=1, source_target_pairs={{0,8},{4,12},{8,0},{12,4},{1,9},{5,13},{9,1},{13,5},{2,10},{6,14},... | collective-permute-start | bytes 786440 | tf_op jit(solution)/shard_map/ppermute | solution.py:43
  37.6 33.6 %copy-start.2 = (bf16[256,2048]{1,0:T(8,128)(2,1)S(1)}, bf16[256,2048]{1,0:T(8,128)(2,1)}, u32[]{:S(2)}) copy-start(bf16[256,2048]{1,0:T(8,128)(2,1)} %param.24) | copy-start | bytes 3145732
  39.6 36.4 %collective-permute-start.20 = (bf16[256,512]{1,0:T(8,128)(2,1)S(1)}, bf16[256,512]{1,0:T(8,128)(2,1)}, u32[]{:S(2)}, u32[]{:S(2)}) collective-permute-start(bf16[256,512]{1,0:T(8,128)(2,1)S(1)} %bitcast.103), channel_id=1, source_target_pairs={{0,12},{4,0},{8,4},{12,8},{1,13},{5,1},{9,5},{13,9},{2,14},{6,2},{... | collective-permute-start | bytes 786440 | tf_op jit(solution)/shard_map/ppermute | solution.py:43
  71.1 6.3 %copy-start.22 = (f32[8,256]{1,0:T(8,128)S(1)}, f32[8,256]{1,0:T(8,128)}, u32[]{:S(2)}) copy-start(f32[8,256]{1,0:T(8,128)} %get-tuple-element.28) | copy-start | bytes 24580
  71.1 6.3 %collective-permute-start.12 = (f32[8,256]{1,0:T(8,128)}, f32[8,256]{1,0:T(8,128)S(1)}, u32[]{:S(2)}, u32[]{:S(2)}) collective-permute-start(f32[8,256]{1,0:T(8,128)} %get-tuple-element.26), channel_id=1, source_target_pairs={{0,12},{4,0},{8,4},{12,8},{1,13},{5,1},{9,5},{13,9},{2,14},{6,2},{... | collective-permute-start | bytes 24584 | tf_op jit(solution)/shard_map/ppermute | solution.py:43
  73.8 28.3 %collective-permute-start.10 = (bf16[256,512]{1,0:T(8,128)(2,1)}, bf16[256,512]{1,0:T(8,128)(2,1)}, u32[]{:S(2)}, u32[]{:S(2)}) collective-permute-start(bf16[256,512]{1,0:T(8,128)(2,1)} %get-tuple-element.23), channel_id=1, source_target_pairs={{0,8},{4,12},{8,0},{12,4},{1,9},{5,13},{9,1},{13,5},{2,10},{6,14},... | collective-permute-start | bytes 786440 | tf_op jit(solution)/shard_map/ppermute | solution.py:43
  73.8 30.0 %collective-permute-start.11 = (bf16[256,512]{1,0:T(8,128)(2,1)}, bf16[256,512]{1,0:T(8,128)(2,1)}, u32[]{:S(2)}, u32[]{:S(2)}) collective-permute-start(bf16[256,512]{1,0:T(8,128)(2,1)} %get-tuple-element.24), channel_id=1, source_target_pairs={{0,4},{4,8},{8,12},{12,0},{1,5},{5,9},{9,13},{13,1},{2,6},{6,10},{... | collective-permute-start | bytes 786440 | tf_op jit(solution)/shard_map/ppermute | solution.py:43
  75.6 28.6 %collective-permute-start.9 = (bf16[256,512]{1,0:T(8,128)(2,1)}, bf16[256,512]{1,0:T(8,128)(2,1)}, u32[]{:S(2)}, u32[]{:S(2)}) collective-permute-start(bf16[256,512]{1,0:T(8,128)(2,1)} %get-tuple-element.22), channel_id=1, source_target_pairs={{0,12},{4,0},{8,4},{12,8},{1,13},{5,1},{9,5},{13,9},{2,14},{6,2},{... | collective-permute-start | bytes 786440 | tf_op jit(solution)/shard_map/ppermute | solution.py:43
  76.0 25.9 %collective-permute-start.13 = (f32[8,256]{1,0:T(8,128)}, f32[8,256]{1,0:T(8,128)S(1)}, u32[]{:S(2)}, u32[]{:S(2)}) collective-permute-start(f32[8,256]{1,0:T(8,128)} %get-tuple-element.27), channel_id=1, source_target_pairs={{0,8},{4,12},{8,0},{12,4},{1,9},{5,13},{9,1},{13,5},{2,10},{6,14},... | collective-permute-start | bytes 24584 | tf_op jit(solution)/shard_map/ppermute | solution.py:43
  77.4 24.5 %copy-start.9 = (f32[8,256]{1,0:T(8,128)}, f32[8,256]{1,0:T(8,128)S(1)}, u32[]{:S(2)}) copy-start(f32[8,256]{1,0:T(8,128)S(1)} %collective-permute-done.12.refs_5_) | copy-start | bytes 24580
  77.4 24.6 %collective-permute-start.14 = (f32[8,256]{1,0:T(8,128)S(1)}, f32[8,256]{1,0:T(8,128)S(1)}, u32[]{:S(2)}, u32[]{:S(2)}) collective-permute-start(f32[8,256]{1,0:T(8,128)S(1)} %copy-done.22), channel_id=1, source_target_pairs={{0,4},{4,8},{8,12},{12,0},{1,5},{5,9},{9,13},{13,1},{2,6},{6,10},{... | collective-permute-start | bytes 24584 | tf_op jit(solution)/shard_map/ppermute | solution.py:43
  81.2 26.9 %copy-start.7 = (f32[2048]{0:T(1024)S(1)}, f32[2048]{0:T(1024)}, u32[]{:S(2)}) copy-start(f32[2048]{0:T(1024)} %param.31) | copy-start | bytes 24580
  101.9 3.6 %copy-start.10 = (f32[8,256]{1,0:T(8,128)}, f32[8,256]{1,0:T(8,128)S(1)}, u32[]{:S(2)}) copy-start(f32[8,256]{1,0:T(8,128)S(1)} %collective-permute-done.13.refs_6_) | copy-start | bytes 24580
  101.9 17.8 %collective-permute-start.21 = (bf16[256,512]{1,0:T(8,128)(2,1)}, bf16[256,512]{1,0:T(8,128)(2,1)}, u32[]{:S(2)}, u32[]{:S(2)}) collective-permute-start(bf16[256,512]{1,0:T(8,128)(2,1)} %get-tuple-element.30), channel_id=1, source_target_pairs={{0,12},{4,0},{8,4},{12,8},{1,13},{5,1},{9,5},{13,9},{2,14},{6,2},{... | collective-permute-start | bytes 786440 | tf_op jit(solution)/shard_map/ppermute | solution.py:43
  102.0 3.6 %copy-start.12 = (f32[8,256]{1,0:T(8,128)}, f32[8,256]{1,0:T(8,128)S(1)}, u32[]{:S(2)}) copy-start(f32[8,256]{1,0:T(8,128)S(1)} %collective-permute-done.14.refs_7_) | copy-start | bytes 24580
  102.0 17.7 %collective-permute-start.22 = (bf16[256,512]{1,0:T(8,128)(2,1)}, bf16[256,512]{1,0:T(8,128)(2,1)}, u32[]{:S(2)}, u32[]{:S(2)}) collective-permute-start(bf16[256,512]{1,0:T(8,128)(2,1)} %get-tuple-element.31), channel_id=1, source_target_pairs={{0,8},{4,12},{8,0},{12,4},{1,9},{5,13},{9,1},{13,5},{2,10},{6,14},... | collective-permute-start | bytes 786440 | tf_op jit(solution)/shard_map/ppermute | solution.py:43
  102.1 17.6 %collective-permute-start.23 = (bf16[256,512]{1,0:T(8,128)(2,1)}, bf16[256,512]{1,0:T(8,128)(2,1)}, u32[]{:S(2)}, u32[]{:S(2)}) collective-permute-start(bf16[256,512]{1,0:T(8,128)(2,1)} %get-tuple-element.32), channel_id=1, source_target_pairs={{0,4},{4,8},{8,12},{12,0},{1,5},{5,9},{9,13},{13,1},{2,6},{6,10},{... | collective-permute-start | bytes 786440 | tf_op jit(solution)/shard_map/ppermute | solution.py:43
  103.8 12.7 %collective-permute-start.24 = (f32[8,256]{1,0:T(8,128)}, f32[8,256]{1,0:T(8,128)S(1)}, u32[]{:S(2)}, u32[]{:S(2)}) collective-permute-start(f32[8,256]{1,0:T(8,128)} %get-tuple-element.34), channel_id=1, source_target_pairs={{0,12},{4,0},{8,4},{12,8},{1,13},{5,1},{9,5},{13,9},{2,14},{6,2},{... | collective-permute-start | bytes 24584 | tf_op jit(solution)/shard_map/ppermute | solution.py:43
  104.2 13.3 %collective-permute-start.25 = (f32[8,256]{1,0:T(8,128)}, f32[8,256]{1,0:T(8,128)S(1)}, u32[]{:S(2)}, u32[]{:S(2)}) collective-permute-start(f32[8,256]{1,0:T(8,128)} %get-tuple-element.35), channel_id=1, source_target_pairs={{0,8},{4,12},{8,0},{12,4},{1,9},{5,13},{9,1},{13,5},{2,10},{6,14},... | collective-permute-start | bytes 24584 | tf_op jit(solution)/shard_map/ppermute | solution.py:43
  108.1 8.4 %copy-start.21 = (f32[8,256]{1,0:T(8,128)S(1)}, f32[8,256]{1,0:T(8,128)}, u32[]{:S(2)}) copy-start(f32[8,256]{1,0:T(8,128)} %get-tuple-element.36) | copy-start | bytes 24580
  116.5 3.2 %copy-start.11 = (f32[8,256]{1,0:T(8,128)}, f32[8,256]{1,0:T(8,128)S(1)}, u32[]{:S(2)}) copy-start(f32[8,256]{1,0:T(8,128)S(1)} %collective-permute-done.24.refs_5_) | copy-start | bytes 24580
  116.5 1.2 collective-permute-start.26
  117.5 11.6 %collective-permute-start.15 = (bf16[64,2048]{1,0:T(8,128)(2,1)}, bf16[64,2048]{1,0:T(8,128)(2,1)}, u32[]{:S(2)}, u32[]{:S(2)}) collective-permute-start(bf16[64,2048]{1,0:T(8,128)(2,1)} %get-tuple-element.44), channel_id=1, source_target_pairs={{0,2},{1,3},{2,0},{3,1},{4,6},{5,7},{6,4},{7,5},{8,10},{9,11},{10,... | collective-permute-start | bytes 786440 | tf_op jit(solution)/shard_map/ppermute | solution.py:43
  117.7 28.2 %collective-permute-start.16 = (bf16[64,2048]{1,0:T(8,128)(2,1)}, bf16[64,2048]{1,0:T(8,128)(2,1)}, u32[]{:S(2)}, u32[]{:S(2)}) collective-permute-start(bf16[64,2048]{1,0:T(8,128)(2,1)} %get-tuple-element.46), channel_id=1, source_target_pairs={{0,1},{1,2},{2,3},{3,0},{4,5},{5,6},{6,7},{7,4},{8,9},{9,10},{10,1... | collective-permute-start | bytes 786440 | tf_op jit(solution)/shard_map/ppermute | solution.py:43
  119.7 35.0 %collective-permute-start.17 = (bf16[64,2048]{1,0:T(8,128)(2,1)S(1)}, bf16[64,2048]{1,0:T(8,128)(2,1)}, u32[]{:S(2)}, u32[]{:S(2)}) collective-permute-start(bf16[64,2048]{1,0:T(8,128)(2,1)S(1)} %get-tuple-element.45), channel_id=1, source_target_pairs={{0,3},{1,0},{2,1},{3,2},{4,7},{5,4},{6,5},{7,6},{8,11},{9,8},{10,9... | collective-permute-start | bytes 786440 | tf_op jit(solution)/shard_map/ppermute | solution.py:43
  124.8 32.2 %collective-permute-start.27 = (bf16[64,2048]{1,0:T(8,128)(2,1)S(1)}, bf16[64,2048]{1,0:T(8,128)(2,1)S(1)}, u32[]{:S(2)}, u32[]{:S(2)}) collective-permute-start(bf16[64,2048]{1,0:T(8,128)(2,1)S(1)} %get-tuple-element.47), channel_id=1, source_target_pairs={{0,2},{1,3},{2,0},{3,1},{4,6},{5,7},{6,4},{7,5},{8,10},{9,11},{10,... | collective-permute-start | bytes 786440 | tf_op jit(solution)/shard_map/ppermute | solution.py:43
  126.4 36.2 %collective-permute-start.28 = (bf16[64,2048]{1,0:T(8,128)(2,1)S(1)}, bf16[64,2048]{1,0:T(8,128)(2,1)S(1)}, u32[]{:S(2)}, u32[]{:S(2)}) collective-permute-start(bf16[64,2048]{1,0:T(8,128)(2,1)S(1)} %get-tuple-element.49), channel_id=1, source_target_pairs={{0,1},{1,2},{2,3},{3,0},{4,5},{5,6},{6,7},{7,4},{8,9},{9,10},{10,1... | collective-permute-start | bytes 786440 | tf_op jit(solution)/shard_map/ppermute | solution.py:43
  129.0 36.8 %collective-permute-start.29 = (bf16[64,2048]{1,0:T(8,128)(2,1)S(1)}, bf16[64,2048]{1,0:T(8,128)(2,1)S(1)}, u32[]{:S(2)}, u32[]{:S(2)}) collective-permute-start(bf16[64,2048]{1,0:T(8,128)(2,1)S(1)} %get-tuple-element.48), channel_id=1, source_target_pairs={{0,3},{1,0},{2,1},{3,2},{4,7},{5,4},{6,5},{7,6},{8,11},{9,8},{10,9... | collective-permute-start | bytes 786440 | tf_op jit(solution)/shard_map/ppermute | solution.py:43
  (5 other events, 11.5 us)

commit v2 on v1

--- a/solution.py
+++ b/solution.py
@@ -43,12 +43,48 @@
     return lax.ppermute(value, axis, [(i, (i + step) % size) for i in range(size)])
 
 
+def passage_planes(store_rows, gain_vec, key_proj, value_proj):
+    total_rows, model_width = store_rows.shape
+    planes = key_proj.shape[1] // 128
+    step_rows = min(256, total_rows)
+
+    def kernel(row_ref, gain_ref, key_w, value_w, key_ref, value_ref):
+        floats = row_ref[...].astype(jnp.float32)
+        inv_scale = lax.rsqrt(jnp.mean(floats * floats, axis=-1, keepdims=True) + EPS)
+        normed = (floats * inv_scale * gain_ref[...]).astype(jnp.bfloat16)
+        for weight, target in ((key_w, key_ref), (value_w, value_ref)):
+            result = jnp.dot(normed, weight[...], preferred_element_type=jnp.float32)
+            for c in range(planes):
+                target[c] = result[:, c * 128 : (c + 1) * 128].astype(jnp.bfloat16)
+
+    whole = pl.BlockSpec(memory_space=pltpu.VMEM)
+    plane_spec = pl.BlockSpec((planes, step_rows, 128), lambda i: (0, i, 0))
+    return pl.pallas_call(
+        kernel,
+        grid=(total_rows // step_rows,),
+        out_shape=[jax.ShapeDtypeStruct((planes, total_rows, 128), jnp.bfloat16)] * 2,
+        in_specs=[pl.BlockSpec((step_rows, model_width), lambda i: (i, 0)), whole, whole, whole],
+        out_specs=[plane_spec, plane_spec],
+        name="passage_planes",
+    )(store_rows, gain_vec[None], key_proj, value_proj)
+
+
+def stat_place(rows, head_width):
+    across = head_width // 128
+    tiles = 3 * (rows // 128)
+    places = [(rows + 8 * (t // across), 128 * (t % across)) for t in range(tiles)]
+    return places, 16 * -(-(-(-tiles // across)) // 2)
+
+
 def owner_attention(me, ids, query_list, keys, values, block_len, per_block, pass_rows):
     sources = len(query_list)
-    rows, head_width = query_list[0].shape
-    blocks = rows // block_len
+    head_width = query_list[0].shape[1]
+    blocks = ids.shape[1] // per_block
+    rows = blocks * block_len
     heads = head_width // HD
-    held = keys.shape[0] // pass_rows
+    held = keys.shape[1] // pass_rows
+    lanes = HD // 128
+    places, extra = stat_place(rows, head_width)
     slots = blocks * per_block + BATCH
     scale = HD ** (-0.5)
     pair = 128 // block_len
@@ -57,8 +93,7 @@
         query_refs = refs[:sources]
         key_ref, value_ref = refs[sources : sources + 2]
         out_refs = refs[sources + 2 : 2 * sources + 2]
-        stat_refs = refs[2 * sources + 2 : 3 * sources + 2]
-        list_block, list_pass, part_ref, top_ref, sum_ref = refs[3 * sources + 2 :]
+        list_block, list_pass, part_ref, top_ref, sum_ref = refs[2 * sources + 2 :]
         first = me_ref[0] * held
         lane = lax.broadcasted_iota(jnp.int32, (block_len, 128), 1)
         for source in range(sources):
@@ -87,8 +122,16 @@
                     for h in range(heads):
                         cols = slice(h * HD, (h + 1) * HD)
                         q = query_ref[pl.ds(block_at, block_len), cols]
-                        k = key_ref[pl.ds(pass_at, pass_rows), cols]
-                        v = value_ref[pl.ds(pass_at, pass_rows), cols]
+                        k, v = (
+                            jnp.concatenate(
+                                [
+                                    ref[h * lanes + c, pl.ds(pass_at, pass_rows), :]
+                                    for c in range(lanes)
+                                ],
+                                axis=1,
+                            )
+                            for ref in (key_ref, value_ref)
+                        )
                         scores = lax.dot_general(
                             q, k, (((1,), (1,)), ((), ())), preferred_element_type=jnp.float32
                         ) * scale
@@ -98,7 +141,10 @@
                         out = jnp.dot(
                             exponent.astype(jnp.bfloat16), v, preferred_element_type=jnp.float32
                         )
-                        part_ref[slot, :, cols] = out.astype(jnp.bfloat16)
+                        for c in range(lanes):
+                            part_ref[slot, h * lanes + c] = out[
+                                :, c * 128 : (c + 1) * 128
+                            ].astype(jnp.bfloat16)
                         top_ref[slot, h] = jnp.broadcast_to(top, (block_len, 128))
                         sum_ref[slot, h] = jnp.broadcast_to(total, (block_len, 128))
                 return carry
@@ -121,55 +167,65 @@
                     for j in range(1, per_block):
                         best = jnp.maximum(best, tops[j])
                     total = jnp.zeros((block_len, 128), jnp.float32)
-                    merged = jnp.zeros((block_len, HD), jnp.float32)
+                    merged = [jnp.zeros((block_len, 128), jnp.float32)] * lanes
                     for j in range(per_block):
                         weight = jnp.where(j < held_here, jnp.exp(tops[j] - best), 0.0)
                         total = total + weight * sum_ref[at[j], h]
-                        wide = jnp.concatenate([weight] * (HD // 128), axis=1)
-                        merged = merged + wide * part_ref[at[j], :, cols].astype(jnp.float32)
+                        merged = [
+                            merged[c]
+                            + weight * part_ref[at[j], h * lanes + c].astype(jnp.float32)
+                            for c in range(lanes)
+                        ]
                     out_refs[source][block * block_len : (block + 1) * block_len, cols] = (
-                        merged.astype(jnp.bfloat16)
+                        jnp.concatenate(merged, axis=1).astype(jnp.bfloat16)
                     )
                     tile = jnp.where(lane == h, best, tile)
                     tile = jnp.where(lane == heads + h, total, tile)
                 tiles.append(tile)
             for at_pair in range(0, blocks, pair):
-                square = jnp.concatenate(tiles[at_pair : at_pair + pair], axis=0)
-                stat_refs[source][:, at_pair * block_len : (at_pair + pair) * block_len] = (
-                    square.T[:8]
-                )
+                rest = jnp.concatenate(tiles[at_pair : at_pair + pair], axis=0).T[:8]
+                for piece in range(3):
+                    row, col = places[piece * (rows // 128) + at_pair // pair]
+                    rounded = rest.astype(jnp.bfloat16)
+                    out_refs[source][row : row + 8, col : col + 128] = rounded
+                    rest = rest - rounded.astype(jnp.float32)
 
     whole = pl.BlockSpec(memory_space=pltpu.VMEM)
     scalar = pl.BlockSpec(memory_space=pltpu.SMEM)
     outs = pl.pallas_call(
         kernel,
-        out_shape=[jax.ShapeDtypeStruct((rows, head_width), jnp.bfloat16)] * sources
-        + [jax.ShapeDtypeStruct((8, rows), jnp.float32)] * sources,
+        out_shape=[jax.ShapeDtypeStruct((rows + extra, head_width), jnp.bfloat16)] * sources,
         in_specs=[scalar, scalar] + [whole] * (sources + 2),
-        out_specs=[whole] * (2 * sources),
+        out_specs=[whole] * sources,
         scratch_shapes=[
             pltpu.SMEM((slots,), jnp.int32),
             pltpu.SMEM((slots,), jnp.int32),
-            pltpu.VMEM((slots, block_len, head_width), jnp.bfloat16),
+            pltpu.VMEM((slots, head_width // 128, block_len, 128), jnp.bfloat16),
             pltpu.VMEM((slots, heads, block_len, 128), jnp.float32),
             pltpu.VMEM((slots, heads, block_len, 128), jnp.float32),
         ],
         name="owner_attention",
     )(me, ids, *query_list, keys, values)
-    return outs[:sources], outs[sources:]
-
-
-def merge_owners(out_list, stat_list):
+    return outs
+
+
+def merge_owners(out_list, rows):
     sources = len(out_list)
-    rows, head_width = out_list[0].shape
+    head_width = out_list[0].shape[1]
     heads = head_width // HD
+    places, _ = stat_place(rows, head_width)
 
     def kernel(*refs):
         out_refs = refs[:sources]
-        stat_refs = refs[sources : 2 * sources]
-        result_ref = refs[2 * sources]
+        result_ref = refs[sources]
         for at in range(0, rows, 128):
-            stats = [ref[:, at : at + 128] for ref in stat_refs]
+            stats = []
+            for ref in out_refs:
+                pieces = []
+                for piece in range(3):
+                    row, col = places[piece * (rows // 128) + at // 128]
+                    pieces.append(ref[row : row + 8, col : col + 128].astype(jnp.float32))
+                stats.append(pieces[2] + pieces[1] + pieces[0])
             best = [stats[0][h : h + 1] for h in range(heads)]
             for s in range(1, sources):
                 best = [jnp.maximum(best[h], stats[s][h : h + 1]) for h in range(heads)]
@@ -198,10 +254,10 @@
     return pl.pallas_call(
         kernel,
         out_shape=jax.ShapeDtypeStruct((rows, head_width), jnp.bfloat16),
-        in_specs=[whole] * (2 * sources),
+        in_specs=[whole] * sources,
         out_specs=whole,
         name="merge_owners",
-    )(*out_list, *stat_list)
+    )(*out_list)
 
 
 def local(
@@ -243,18 +299,22 @@
     queries = jnp.dot(
         rms_rows(tokens, query_gain), query_proj, preferred_element_type=jnp.float32
     ).astype(jnp.bfloat16)
-    id_list = [passage_ids] + [shifted(passage_ids, "st", k) for k in steps]
-    all_ids = jnp.stack(id_list)
+    assert owners * pass_local <= 256
     query_chunks = []
+    id_chunks = []
     for c in range(chunks):
-        own = cut(queries, c)
-        query_chunks.append([own] + [shifted(own, "st", k) for k in steps])
-    normed_store = rms_rows(store.reshape(pass_local * pass_rows, model_width), passage_gain)
-    key_rows = jnp.dot(normed_store, key_proj, preferred_element_type=jnp.float32).astype(
-        jnp.bfloat16
-    )
-    value_rows = jnp.dot(normed_store, value_proj, preferred_element_type=jnp.float32).astype(
-        jnp.bfloat16
+        ids = passage_ids.reshape(shards, chunks, -1)[:, c].reshape(1, -1)
+        id_rows = jnp.pad(
+            ids.astype(jnp.bfloat16), ((0, 15), (0, head_width - ids.shape[1]))
+        )
+        own = jnp.concatenate([cut(queries, c), id_rows], axis=0)
+        query_list = [own] + [shifted(own, "st", k) for k in steps]
+        query_chunks.append(query_list)
+        id_chunks.append(
+            jnp.stack([q[shards * run, : ids.shape[1]] for q in query_list]).astype(jnp.int32)
+        )
+    key_planes, value_planes = passage_planes(
+        store.reshape(pass_local * pass_rows, model_width), passage_gain, key_proj, value_proj
     )
     mix_input = rms_rows(tokens, mix_gain)
     value_part = jnp.dot(mix_input, glu_value, preferred_element_type=jnp.float32)
@@ -269,18 +329,17 @@
         channel_total = channel_total + shifted(sums, "tp", k)
     answers = []
     for c in range(chunks):
-        ids = all_ids.reshape(
-            owners, shards, chunks, blocks_per_shard // chunks * per_block
-        )[:, :, c].reshape(owners, -1)
-        out_list, stat_list = owner_attention(
-            me[None], ids, query_chunks[c], key_rows, value_rows, block_len, per_block, pass_rows
+        out_list = owner_attention(
+            me[None],
+            id_chunks[c],
+            query_chunks[c],
+            key_planes,
+            value_planes,
+            block_len,
+            per_block,
+            pass_rows,
         )
-        answers.append(
-            (
-                [out_list[0]] + [shifted(out_list[k], "st", -k) for k in steps],
-                [stat_list[0]] + [shifted(stat_list[k], "st", -k) for k in steps],
-            )
-        )
+        answers.append([out_list[0]] + [shifted(out_list[k], "st", -k) for k in steps])
     row_mean = channel_total[0] / CA
     row_var = channel_total[1] / CA - row_mean * row_mean
     activation = jax.nn.silu(
@@ -288,7 +347,7 @@
     ).astype(jnp.bfloat16)
     results = []
     for c in range(chunks):
-        attended = merge_owners(*answers[c])
+        attended = merge_owners(answers[c], shards * run)
         conv_term = jnp.dot(cut(activation, c), mix_out, preferred_element_type=jnp.float32)
         attn_term = jnp.dot(attended, attn_out, preferred_element_type=jnp.float32)
         partial = (

time: 166 us -> 150 us (0.904); the launches traced: 167 us -> 148 us
  starting transfers between devices: 36.6 us -> 18.8 us
  Pallas kernels: 52.6 us -> 63.9 us
  matrix products: 22.5 us -> 14.9 us
  other arithmetic: 13 us -> 10.7 us
  waiting for transfers between devices: 36.1 us -> 34.2 us
    ppermute x30 -> x21, starting transfers between devices: 36.6 us -> 18.8 us  [shifted(): lax.ppermute(value, axis, [(i, (i + step) % size) for i in range(size)])]
    pallas_call x2 -> x3, Pallas kernels: 47.5 us -> 58.9 us  [the longest x2 49.4 us: owner_attention(): pl.pallas_call(kernel, out_shape=[jax.ShapeDtypeStruct((rows + extra, hea...]
    dot_general x2 -> x0, matrix products: 6.69 us -> none  [the longest x1 3.35 us: local(): jnp.dot(normed_store, key_proj, preferred_element_type=jnp.float32)]
    slice x1 -> x7, local copies, waits for them, and re-layouts: 0.06 us -> 3.93 us  [the longest x6 3.9 us: local(): q[shards * run, :ids.shape[1]]]
    reduce_sum x2 -> x1, other arithmetic: 5.3 us -> 2.23 us  [rms_rows(): jnp.mean(floats * floats, axis=-1, keepdims=True) + EPS]
    ppermute x30 -> x21, waiting for transfers between devices: 36.1 us -> 34.2 us  [shifted(): lax.ppermute(value, axis, [(i, (i + step) % size) for i in range(size)])]
  transfers between devices with their start and end apart: 30 -> 21, of which waited for: 8 -> 7; matrix products, arithmetic and copies ran while one was open for 23% -> 16% of each run, Pallas kernels for 32% -> 43%
where the time goes in v2:
time: 150 us; the launch traced here: 148 us
  Pallas kernels  63.9 us (43%)
  waiting for transfers between devices  34.2 us (23%)
  starting transfers between devices  18.8 us (13%)
  matrix products  14.9 us (10%)
  other arithmetic  10.7 us (7%)
  local copies, waits for them, and re-layouts  5.58 us (4%)
    pallas_call x2, Pallas kernels, owner_attention(): pl.pallas_call(kernel, out_shape=[jax.ShapeDtypeStruct((rows + extra, hea...  49.4 us
    ppermute x21, waiting for transfers between devices, shifted(): lax.ppermute(value, axis, [(i, (i + step) % size) for i in range(size)])  34.2 us
    ppermute x21, starting transfers between devices, shifted(): lax.ppermute(value, axis, [(i, (i + step) % size) for i in range(size)])  18.8 us
    pallas_call x1, Pallas kernels, passage_planes(): pl.pallas_call(kernel, grid=(total_rows // step_rows,), out_shape=[jax.Sh...  9.46 us
    pallas_call x2, Pallas kernels, merge_owners(): pl.pallas_call(kernel, out_shape=jax.ShapeDtypeStruct((rows, head_width),...  5.06 us
    dot_general x2, matrix products, local(): attn_term = jnp.dot(attended, attn_out, preferred_element_type=jnp.float32)  4.81 us
    slice x6, local copies, waits for them, and re-layouts, local(): q[shards * run, :ids.shape[1]]  3.9 us
    dot_general x2, matrix products, local(): jnp.dot(cut(activation, c), mix_out, preferred_element_type=jnp.float32)  3.53 us
  transfers between devices with their start and end apart: 21, of which 7 were waited for; matrix products, arithmetic and copies ran while one was open for 16% of the time, Pallas kernels for 43%

profile of v2, /device:TPU:9, one launch (start us, length us, event | category | flops | bytes accessed | tf_op | source)
XLA Modules:
  0.0 148.4 jit_solution(8231060045291093863)
XLA Ops:
  0.0 2.2 %fusion.4 = f32[512]{0:T(512)S(1)} fusion(bf16[512,2048]{1,0:T(8,128)(2,1)} %param.16), kind=kLoop, calls=%fused_computation.6 | loop fusion | flops 3145216 | bytes 2099200 | tf_op jit(solution)/shard_map/reduce_sum | solution.py:18
  2.4 3.0 %fusion.13 = bf16[512,512]{1,0:T(8,128)(2,1)S(1)} fusion(bf16[2048,512]{1,0:T(8,128)(2,1)} %param.27, bf16[512,2048]{1,0:T(8,128)(2,1)S(1)} %copy-done.2, f32[2048]{0:T(1024)} %param.25, f32[512]{0:T(512)S(1)} %add_rsqrt_fusion.1), kind=kOutput, calls=%fused_computation.46 | convolution fusion | flops 1078198272 | bytes 4728832 | tf_op jit(solution)/shard_map/dot_general | solution.py:299
  5.6 1.8 %collective-permute-start.3 = (bf16[272,512]{1,0:T(8,128)(2,1)S(1)}, bf16[272,512]{1,0:T(8,128)(2,1)}, u32[]{:S(2)}, u32[]{:S(2)}) collective-permute-start(bf16[272,512]{1,0:T(8,128)(2,1)S(1)} %fusion.90.refs_0_), channel_id=1, source_target_pairs={{0,4},{4,8},{8,12},{12,0},{1,5},{5,9},{9,13},{13,1},{2,6},{6,10},{... | collective-permute-start | bytes 835592 | tf_op jit(solution)/shard_map/ppermute | solution.py:43
  7.8 2.8 %fusion.18 = f32[512,256]{1,0:T(8,128)S(1)} fusion(bf16[2048,256]{1,0:T(8,128)(2,1)} %param.21, bf16[512,2048]{1,0:T(8,128)(2,1)} %param.16, f32[2048]{0:T(1024)S(1)} %copy-done.15, f32[512]{0:T(512)S(1)} %add_rsqrt_fusion.1), kind=kOutput, calls=%fused_computation.51 | convolution fusion | flops 541458432 | bytes 3680256 | tf_op jit(solution)/shard_map/dot_general | solution.py:321
  10.6 0.8 bitcast_convert_fusion
  11.4 2.9 %fusion.94 = (f32[4,128]{1,0:T(4,128)S(1)}, f32[4,128]{1,0:T(4,128)S(1)}, f32[4,128,256]{2,1,0:T(8,128)}) fusion(f32[256]{0:T(256)S(1)} %bitcast.129, f32[256]{0:T(256)S(1)} %bitcast.130, f32[256]{0:T(256)S(1)} %bitcast.101, f32[256]{0:T(256)S(1)} %bitcast.102, f32[256]{0:T(256)S(1)} %bitcast.103, f32[256]{0:T(256)S(1)} %bitcast.104, f32[256]{0:T(256)S(1)} %bitcast.105, ...), kind=kLoop, calls=%fused_computation.178 | loop fusion | flops 8387584 | bytes 1084416 | tf_op jit(solution)/shard_map/reduce_sum | solution.py:326
  14.4 1.3 collective-permute-start
  15.7 1.1 collective-permute-start.1
  16.8 1.4 collective-permute-start.2
  18.3 0.8 fusion.91.refs_0_
  19.0 9.5 %passage_planes.1 = (bf16[4,1024,128]{2,1,0:T(8,128)(2,1)}, bf16[4,1024,128]{2,1,0:T(8,128)(2,1)}) custom-call(bf16[1024,2048]{1,0:T(8,128)(2,1)} %bitcast.83, f32[1,2048]{1,0:T(1,128)} %bitcast.99, bf16[2048,512]{1,0:T(8,128)(2,1)} %key_w.1, bf16[2048,512]{1,0:T(8,128)(2,1)} %value_w.1), custom_call_target="tpu_custom_call" | custom-call | tf_op jit(solution)/shard_map/passage_planes/pallas_call | solution.py:62
  28.5 1.1 collective-permute-start.5
  29.7 0.7 collective-permute-start.12
  30.3 1.2 collective-permute-start.13
  31.8 1.3 multiply_convert_fusion
  33.1 1.8 %fusion.98 = f32[256,2048]{1,0:T(8,128)} fusion(bf16[256,256]{1,0:T(8,128)(2,1)S(1)} %bitcast.93, bf16[256,2048]{1,0:T(8,128)(2,1)S(1)} %copy-done.1), kind=kOutput, calls=%fused_computation.182 | convolution fusion | flops 268435456 | bytes 3276800 | tf_op jit(solution)/shard_map/dot_general | solution.py:351
  34.9 0.6 slice.310
  35.5 0.7 slice.311
  36.2 0.6 collective-permute-done.5.refs_3_
  36.8 0.7 slice.312
  37.4 0.6 maximum_convert_fusion.ids_ref
  38.0 26.7 %owner_attention.2 = (bf16[272,512]{1,0:T(8,128)(2,1)}, bf16[272,512]{1,0:T(8,128)(2,1)}, bf16[272,512]{1,0:T(8,128)(2,1)}, bf16[272,512]{1,0:T(8,128)(2,1)}) custom-call(s32[1]{0:T(128)} %bitcast.37.me_ref, s32[4,16]{1,0:T(4,128)} %maximum_convert_fusion.ids_ref, bf16[272,512]{1,0:T(8,128)(2,1)} %copy-done.4, ...), custom_call_target="tpu_custom_call" | custom-call | tf_op jit(solution)/shard_map/owner_attention/pallas_call | solution.py:195
  64.8 1.7 %collective-permute-start.8 = (bf16[272,512]{1,0:T(8,128)(2,1)}, bf16[272,512]{1,0:T(8,128)(2,1)}, u32[]{:S(2)}, u32[]{:S(2)}) collective-permute-start(bf16[272,512]{1,0:T(8,128)(2,1)} %get-tuple-element.20), channel_id=1, source_target_pairs={{0,4},{4,8},{8,12},{12,0},{1,5},{5,9},{9,13},{13,1},{2,6},{6,10},{... | collective-permute-start | bytes 835592 | tf_op jit(solution)/shard_map/ppermute | solution.py:43
  66.5 1.8 %fusion.99 = f32[256,2048]{1,0:T(8,128)} fusion(bf16[256,256]{1,0:T(8,128)(2,1)S(1)} %bitcast.92, bf16[256,2048]{1,0:T(8,128)(2,1)S(1)} %copy-done.1), kind=kOutput, calls=%fused_computation.183 | convolution fusion | flops 268435456 | bytes 3276800 | tf_op jit(solution)/shard_map/dot_general | solution.py:351
  68.3 0.7 slice.316
  68.9 0.7 slice.317
  69.6 0.6 slice.318
  70.2 0.6 maximum_convert_fusion.1.ids_ref
  70.8 22.7 %owner_attention.3 = (bf16[272,512]{1,0:T(8,128)(2,1)}, bf16[272,512]{1,0:T(8,128)(2,1)}, bf16[272,512]{1,0:T(8,128)(2,1)}, bf16[272,512]{1,0:T(8,128)(2,1)}) custom-call(s32[1]{0:T(128)} %bitcast.37.me_ref, s32[4,16]{1,0:T(4,128)} %maximum_convert_fusion.1.ids_ref, bf16[272,512]{1,0:T(8,128)(2,1)} %fusion.91.refs_0_, ...), custom_call_target="tpu_custom_call" | custom-call | tf_op jit(solution)/shard_map/owner_attention/pallas_call | solution.py:195
  93.6 1.8 %collective-permute-start.17 = (bf16[272,512]{1,0:T(8,128)(2,1)}, bf16[272,512]{1,0:T(8,128)(2,1)}, u32[]{:S(2)}, u32[]{:S(2)}) collective-permute-start(bf16[272,512]{1,0:T(8,128)(2,1)} %get-tuple-element.24), channel_id=1, source_target_pairs={{0,4},{4,8},{8,12},{12,0},{1,5},{5,9},{9,13},{13,1},{2,6},{6,10},{... | collective-permute-start | bytes 835592 | tf_op jit(solution)/shard_map/ppermute | solution.py:43
  95.3 2.5 %merge_owners.2 = bf16[256,512]{1,0:T(8,128)(2,1)} custom-call(bf16[272,512]{1,0:T(8,128)(2,1)} %get-tuple-element.17.refs_0_, bf16[272,512]{1,0:T(8,128)(2,1)} %copy-done.5, bf16[272,512]{1,0:T(8,128)(2,1)} %collective-permute-done.7.refs_2_, bf16[272,512]{1,0:T(8,128)(2,1)} %collective-permute-done.8.refs_3_), custom_call_target="tpu_custom_call" | custom-call | tf_op jit(solution)/shard_map/merge_owners/pallas_call | solution.py:254
  97.9 2.4 %fusion.7 = bf16[256,2048]{1,0:T(8,128)(2,1)S(1)} fusion(f32[256,2048]{1,0:T(8,128)} %fusion.98, bf16[256,512]{1,0:T(8,128)(2,1)} %merge_owners.2, bf16[512,2048]{1,0:T(8,128)(2,1)S(1)} %copy-done, f32[2048]{0:T(1024)S(1)} %copy-done.7), kind=kOutput, calls=%fused_computation.11 | convolution fusion | flops 538443776 | bytes 5513216 | tf_op jit(solution)/shard_map/dot_general | solution.py:352
  100.3 0.9 dynamic-slice_bitcast_fusion.5
  101.3 1.4 collective-permute-start.11
  102.7 0.4 collective-permute-done.15.refs_1_
  103.1 1.3 collective-permute-start.9
  104.4 2.5 %merge_owners.3 = bf16[256,512]{1,0:T(8,128)(2,1)} custom-call(bf16[272,512]{1,0:T(8,128)(2,1)} %get-tuple-element.21.refs_0_, bf16[272,512]{1,0:T(8,128)(2,1)} %collective-permute-done.15.refs_1_, bf16[272,512]{1,0:T(8,128)(2,1)} %collective-permute-done.16.refs_2_, bf16[272,512]{1,0:T(8,128)(2,1)} %collective-permute-done.17.refs_3_), custom_call_target="tpu_custom_call" | custom-call | tf_op jit(solution)/shard_map/merge_owners/pallas_call | solution.py:254
  106.9 2.4 %fusion.8 = bf16[256,2048]{1,0:T(8,128)(2,1)S(1)} fusion(f32[256,2048]{1,0:T(8,128)} %fusion.99, bf16[256,512]{1,0:T(8,128)(2,1)} %merge_owners.3, bf16[512,2048]{1,0:T(8,128)(2,1)S(1)} %copy-done, f32[2048]{0:T(1024)S(1)} %copy-done.7), kind=kOutput, calls=%fused_computation.12 | convolution fusion | flops 538443776 | bytes 5513216 | tf_op jit(solution)/shard_map/dot_general | solution.py:352
  109.4 1.1 collective-permute-start.18
  110.5 1.3 collective-permute-start.19
  111.9 1.1 collective-permute-start.20
  113.0 0.8 collective-permute-done.11
  113.8 14.9 %collective-permute-done.9 = bf16[64,2048]{1,0:T(8,128)(2,1)} collective-permute-done((bf16[64,2048]{1,0:T(8,128)(2,1)}, bf16[64,2048]{1,0:T(8,128)(2,1)}, u32[]{:S(2)}, u32[]{:S(2)}) %collective-permute-start.9) | collective-permute-done | bytes 262176 | tf_op jit(solution)/shard_map/ppermute | solution.py:43
  128.6 1.2 fusion.89
  129.8 10.0 %collective-permute-done.18 = bf16[64,2048]{1,0:T(8,128)(2,1)S(1)} collective-permute-done((bf16[64,2048]{1,0:T(8,128)(2,1)S(1)}, bf16[64,2048]{1,0:T(8,128)(2,1)S(1)}, u32[]{:S(2)}, u32[]{:S(2)}) %collective-permute-start.18) | collective-permute-done | bytes 262176 | tf_op jit(solution)/shard_map/ppermute | solution.py:43
  139.8 5.6 %collective-permute-done.19 = bf16[64,2048]{1,0:T(8,128)(2,1)S(1)} collective-permute-done((bf16[64,2048]{1,0:T(8,128)(2,1)S(1)}, bf16[64,2048]{1,0:T(8,128)(2,1)S(1)}, u32[]{:S(2)}, u32[]{:S(2)}) %collective-permute-start.19) | collective-permute-done | bytes 262176 | tf_op jit(solution)/shard_map/ppermute | solution.py:43
  145.4 2.0 %collective-permute-done.20 = bf16[64,2048]{1,0:T(8,128)(2,1)S(1)} collective-permute-done((bf16[64,2048]{1,0:T(8,128)(2,1)S(1)}, bf16[64,2048]{1,0:T(8,128)(2,1)S(1)}, u32[]{:S(2)}, u32[]{:S(2)}) %collective-permute-start.20) | collective-permute-done | bytes 262176 | tf_op jit(solution)/shard_map/ppermute | solution.py:43
  147.5 0.8 pad_maximum_fusion
  (72 shorter events, 1.4 us)
Async XLA Ops:
  0.0 97.9 %copy-start = (bf16[512,2048]{1,0:T(8,128)(2,1)S(1)}, bf16[512,2048]{1,0:T(8,128)(2,1)}, u32[]{:S(2)}) copy-start(bf16[512,2048]{1,0:T(8,128)(2,1)} %param.30) | copy-start | bytes 6291460
  0.0 2.4 %copy-start.2 = (bf16[512,2048]{1,0:T(8,128)(2,1)S(1)}, bf16[512,2048]{1,0:T(8,128)(2,1)}, u32[]{:S(2)}) copy-start(bf16[512,2048]{1,0:T(8,128)(2,1)} %param.16) | copy-start | bytes 6291460
  2.4 3.0 %copy-start.12 = (s32[8,4]{0,1:T(4,128)S(1)}, s32[8,4]{0,1:T(4,128)}, u32[]{:S(2)}) copy-start(s32[8,4]{0,1:T(4,128)} %param.18) | copy-start | bytes 388
  2.4 5.3 %copy-start.6 = (bf16[31,256]{1,0:T(8,128)(2,1)S(1)}, bf16[31,256]{1,0:T(8,128)(2,1)}, u32[]{:S(2)}) copy-start(bf16[31,256]{1,0:T(8,128)(2,1)} %param.22) | copy-start | bytes 47620
  2.4 5.4 %copy-start.15 = (f32[2048]{0:T(1024)S(1)}, f32[2048]{0:T(1024)}, u32[]{:S(2)}) copy-start(f32[2048]{0:T(1024)} %param.19) | copy-start | bytes 24580
  5.6 2.2 %copy-start.8 = (bf16[1,16]{1,0:T(2,128)(2,1)}, bf16[1,16]{1,0:T(2,128)(2,1)S(1)}, u32[]{:S(2)}) copy-start(bf16[1,16]{1,0:T(2,128)(2,1)S(1)} %convert_element_type.481) | copy-start | bytes 100
  5.6 22.9 %copy-start.4 = (bf16[272,512]{1,0:T(8,128)(2,1)}, bf16[272,512]{1,0:T(8,128)(2,1)S(1)}, u32[]{:S(2)}) copy-start(bf16[272,512]{1,0:T(8,128)(2,1)S(1)} %fusion.90.refs_0_) | copy-start | bytes 835588
  5.6 29.2 %collective-permute-start.3 = (bf16[272,512]{1,0:T(8,128)(2,1)S(1)}, bf16[272,512]{1,0:T(8,128)(2,1)}, u32[]{:S(2)}, u32[]{:S(2)}) collective-permute-start(bf16[272,512]{1,0:T(8,128)(2,1)S(1)} %fusion.90.refs_0_), channel_id=1, source_target_pairs={{0,4},{4,8},{8,12},{12,0},{1,5},{5,9},{9,13},{13,1},{2,6},{6,10},{... | collective-permute-start | bytes 835592 | tf_op jit(solution)/shard_map/ppermute | solution.py:43
  7.5 28.0 %collective-permute-start.4 = (bf16[272,512]{1,0:T(8,128)(2,1)S(1)}, bf16[272,512]{1,0:T(8,128)(2,1)}, u32[]{:S(2)}, u32[]{:S(2)}) collective-permute-start(bf16[272,512]{1,0:T(8,128)(2,1)S(1)} %fusion.90.refs_0_), channel_id=1, source_target_pairs={{0,8},{4,12},{8,0},{12,4},{1,9},{5,13},{9,1},{13,5},{2,10},{6,14},... | collective-permute-start | bytes 835592 | tf_op jit(solution)/shard_map/ppermute | solution.py:43
  7.8 2.8 %copy-start.3 = (bf16[512,2048]{1,0:T(8,128)(2,1)S(1)}, bf16[512,2048]{1,0:T(8,128)(2,1)}, u32[]{:S(2)}) copy-start(bf16[512,2048]{1,0:T(8,128)(2,1)} %param.16) | copy-start | bytes 6291460
  7.8 2.8 %copy-start.14 = (bf16[2048,256]{1,0:T(8,128)(2,1)S(1)}, bf16[2048,256]{1,0:T(8,128)(2,1)}, u32[]{:S(2)}) copy-start(bf16[2048,256]{1,0:T(8,128)(2,1)} %param.20) | copy-start | bytes 3145732
  14.4 14.1 %collective-permute-start = (f32[2,512]{1,0:T(2,128)S(1)}, f32[2,512]{1,0:T(2,128)S(1)}, u32[]{:S(2)}, u32[]{:S(2)}) collective-permute-start(f32[2,512]{1,0:T(2,128)S(1)} %pad_maximum_fusion.1), channel_id=1, source_target_pairs={{0,1},{1,2},{2,3},{3,0},{4,5},{5,6},{6,7},{7,4},{8,9},{9,10},{10,1... | collective-permute-start | bytes 12296 | tf_op jit(solution)/shard_map/ppermute | solution.py:43
  15.7 14.0 %collective-permute-start.1 = (f32[2,512]{1,0:T(2,128)S(1)}, f32[2,512]{1,0:T(2,128)S(1)}, u32[]{:S(2)}, u32[]{:S(2)}) collective-permute-start(f32[2,512]{1,0:T(2,128)S(1)} %pad_maximum_fusion.1), channel_id=1, source_target_pairs={{0,2},{1,3},{2,0},{3,1},{4,6},{5,7},{6,4},{7,5},{8,10},{9,11},{10,... | collective-permute-start | bytes 12296 | tf_op jit(solution)/shard_map/ppermute | solution.py:43
  16.8 13.5 %collective-permute-start.2 = (f32[2,512]{1,0:T(2,128)S(1)}, f32[2,512]{1,0:T(2,128)S(1)}, u32[]{:S(2)}, u32[]{:S(2)}) collective-permute-start(f32[2,512]{1,0:T(2,128)S(1)} %pad_maximum_fusion.1), channel_id=1, source_target_pairs={{0,3},{1,0},{2,1},{3,2},{4,7},{5,4},{6,5},{7,6},{8,11},{9,8},{10,9... | collective-permute-start | bytes 12296 | tf_op jit(solution)/shard_map/ppermute | solution.py:43
  18.3 0.8 copy-start.10
  19.0 12.7 %copy-start.13 = (f32[256]{0:T(256)S(1)}, f32[256]{0:T(256)}, u32[]{:S(2)}) copy-start(f32[256]{0:T(256)} %param.23) | copy-start | bytes 3076
  28.5 4.6 %copy-start.1 = (bf16[256,2048]{1,0:T(8,128)(2,1)S(1)}, bf16[256,2048]{1,0:T(8,128)(2,1)}, u32[]{:S(2)}) copy-start(bf16[256,2048]{1,0:T(8,128)(2,1)} %param.24) | copy-start | bytes 3145732
  28.5 8.2 %collective-permute-start.5 = (bf16[272,512]{1,0:T(8,128)(2,1)S(1)}, bf16[272,512]{1,0:T(8,128)(2,1)}, u32[]{:S(2)}, u32[]{:S(2)}) collective-permute-start(bf16[272,512]{1,0:T(8,128)(2,1)S(1)} %fusion.90.refs_0_), channel_id=1, source_target_pairs={{0,12},{4,0},{8,4},{12,8},{1,13},{5,1},{9,5},{13,9},{2,14},{6,2},{... | collective-permute-start | bytes 835592 | tf_op jit(solution)/shard_map/ppermute | solution.py:43
  29.7 35.1 %collective-permute-start.12 = (bf16[272,512]{1,0:T(8,128)(2,1)}, bf16[272,512]{1,0:T(8,128)(2,1)}, u32[]{:S(2)}, u32[]{:S(2)}) collective-permute-start(bf16[272,512]{1,0:T(8,128)(2,1)} %fusion.91.refs_0_), channel_id=1, source_target_pairs={{0,4},{4,8},{8,12},{12,0},{1,5},{5,9},{9,13},{13,1},{2,6},{6,10},{... | collective-permute-start | bytes 835592 | tf_op jit(solution)/shard_map/ppermute | solution.py:43
  30.3 38.6 %collective-permute-start.13 = (bf16[272,512]{1,0:T(8,128)(2,1)}, bf16[272,512]{1,0:T(8,128)(2,1)}, u32[]{:S(2)}, u32[]{:S(2)}) collective-permute-start(bf16[272,512]{1,0:T(8,128)(2,1)} %fusion.91.refs_0_), channel_id=1, source_target_pairs={{0,8},{4,12},{8,0},{12,4},{1,9},{5,13},{9,1},{13,5},{2,10},{6,14},... | collective-permute-start | bytes 835592 | tf_op jit(solution)/shard_map/ppermute | solution.py:43
  33.1 4.3 %copy-start.9 = (bf16[1,16]{1,0:T(2,128)(2,1)S(1)}, bf16[1,16]{1,0:T(2,128)(2,1)}, u32[]{:S(2)}) copy-start(bf16[1,16]{1,0:T(2,128)(2,1)} %copy-done.8) | copy-start | bytes 100
  34.9 34.7 %collective-permute-start.14 = (bf16[272,512]{1,0:T(8,128)(2,1)}, bf16[272,512]{1,0:T(8,128)(2,1)}, u32[]{:S(2)}, u32[]{:S(2)}) collective-permute-start(bf16[272,512]{1,0:T(8,128)(2,1)} %fusion.91.refs_0_), channel_id=1, source_target_pairs={{0,12},{4,0},{8,4},{12,8},{1,13},{5,1},{9,5},{13,9},{2,14},{6,2},{... | collective-permute-start | bytes 835592 | tf_op jit(solution)/shard_map/ppermute | solution.py:43
  64.7 5.5 %copy-start.11 = (bf16[1,16]{1,0:T(2,128)(2,1)S(1)}, bf16[1,16]{1,0:T(2,128)(2,1)}, u32[]{:S(2)}) copy-start(bf16[1,16]{1,0:T(2,128)(2,1)} %copy-done.10) | copy-start | bytes 100
  64.7 28.8 %collective-permute-start.6 = (bf16[272,512]{1,0:T(8,128)(2,1)}, bf16[272,512]{1,0:T(8,128)(2,1)S(1)}, u32[]{:S(2)}, u32[]{:S(2)}) collective-permute-start(bf16[272,512]{1,0:T(8,128)(2,1)} %get-tuple-element.18), channel_id=1, source_target_pairs={{0,12},{4,0},{8,4},{12,8},{1,13},{5,1},{9,5},{13,9},{2,14},{6,2},{... | collective-permute-start | bytes 835592 | tf_op jit(solution)/shard_map/ppermute | solution.py:43
  64.7 30.6 %collective-permute-start.7 = (bf16[272,512]{1,0:T(8,128)(2,1)}, bf16[272,512]{1,0:T(8,128)(2,1)}, u32[]{:S(2)}, u32[]{:S(2)}) collective-permute-start(bf16[272,512]{1,0:T(8,128)(2,1)} %get-tuple-element.19), channel_id=1, source_target_pairs={{0,8},{4,12},{8,0},{12,4},{1,9},{5,13},{9,1},{13,5},{2,10},{6,14},... | collective-permute-start | bytes 835592 | tf_op jit(solution)/shard_map/ppermute | solution.py:43
  64.8 30.5 %collective-permute-start.8 = (bf16[272,512]{1,0:T(8,128)(2,1)}, bf16[272,512]{1,0:T(8,128)(2,1)}, u32[]{:S(2)}, u32[]{:S(2)}) collective-permute-start(bf16[272,512]{1,0:T(8,128)(2,1)} %get-tuple-element.20), channel_id=1, source_target_pairs={{0,4},{4,8},{8,12},{12,0},{1,5},{5,9},{9,13},{13,1},{2,6},{6,10},{... | collective-permute-start | bytes 835592 | tf_op jit(solution)/shard_map/ppermute | solution.py:43
  70.8 27.0 %copy-start.7 = (f32[2048]{0:T(1024)S(1)}, f32[2048]{0:T(1024)}, u32[]{:S(2)}) copy-start(f32[2048]{0:T(1024)} %param.31) | copy-start | bytes 24580
  93.5 9.6 %collective-permute-start.15 = (bf16[272,512]{1,0:T(8,128)(2,1)}, bf16[272,512]{1,0:T(8,128)(2,1)}, u32[]{:S(2)}, u32[]{:S(2)}) collective-permute-start(bf16[272,512]{1,0:T(8,128)(2,1)} %get-tuple-element.22), channel_id=1, source_target_pairs={{0,12},{4,0},{8,4},{12,8},{1,13},{5,1},{9,5},{13,9},{2,14},{6,2},{... | collective-permute-start | bytes 835592 | tf_op jit(solution)/shard_map/ppermute | solution.py:43
  93.5 10.8 %collective-permute-start.16 = (bf16[272,512]{1,0:T(8,128)(2,1)}, bf16[272,512]{1,0:T(8,128)(2,1)}, u32[]{:S(2)}, u32[]{:S(2)}) collective-permute-start(bf16[272,512]{1,0:T(8,128)(2,1)} %get-tuple-element.23), channel_id=1, source_target_pairs={{0,8},{4,12},{8,0},{12,4},{1,9},{5,13},{9,1},{13,5},{2,10},{6,14},... | collective-permute-start | bytes 835592 | tf_op jit(solution)/shard_map/ppermute | solution.py:43
  93.5 1.8 %copy-start.5 = (bf16[272,512]{1,0:T(8,128)(2,1)}, bf16[272,512]{1,0:T(8,128)(2,1)S(1)}, u32[]{:S(2)}) copy-start(bf16[272,512]{1,0:T(8,128)(2,1)S(1)} %collective-permute-done.6.refs_1_) | copy-start | bytes 835588
  93.6 10.8 %collective-permute-start.17 = (bf16[272,512]{1,0:T(8,128)(2,1)}, bf16[272,512]{1,0:T(8,128)(2,1)}, u32[]{:S(2)}, u32[]{:S(2)}) collective-permute-start(bf16[272,512]{1,0:T(8,128)(2,1)} %get-tuple-element.24), channel_id=1, source_target_pairs={{0,4},{4,8},{8,12},{12,0},{1,5},{5,9},{9,13},{13,1},{2,6},{6,10},{... | collective-permute-start | bytes 835592 | tf_op jit(solution)/shard_map/ppermute | solution.py:43
  101.2 10.7 %collective-permute-start.10 = (bf16[64,2048]{1,0:T(8,128)(2,1)}, bf16[64,2048]{1,0:T(8,128)(2,1)S(1)}, u32[]{:S(2)}, u32[]{:S(2)}) collective-permute-start(bf16[64,2048]{1,0:T(8,128)(2,1)} %get-tuple-element.34), channel_id=1, source_target_pairs={{0,1},{1,2},{2,3},{3,0},{4,5},{5,6},{6,7},{7,4},{8,9},{9,10},{10,1... | collective-permute-start | bytes 786440 | tf_op jit(solution)/shard_map/ppermute | solution.py:43
  101.3 12.5 %collective-permute-start.11 = (bf16[64,2048]{1,0:T(8,128)(2,1)}, bf16[64,2048]{1,0:T(8,128)(2,1)}, u32[]{:S(2)}, u32[]{:S(2)}) collective-permute-start(bf16[64,2048]{1,0:T(8,128)(2,1)} %get-tuple-element.33), channel_id=1, source_target_pairs={{0,3},{1,0},{2,1},{3,2},{4,7},{5,4},{6,5},{7,6},{8,11},{9,8},{10,9... | collective-permute-start | bytes 786440 | tf_op jit(solution)/shard_map/ppermute | solution.py:43
  103.1 25.5 %collective-permute-start.9 = (bf16[64,2048]{1,0:T(8,128)(2,1)}, bf16[64,2048]{1,0:T(8,128)(2,1)}, u32[]{:S(2)}, u32[]{:S(2)}) collective-permute-start(bf16[64,2048]{1,0:T(8,128)(2,1)} %get-tuple-element.32), channel_id=1, source_target_pairs={{0,2},{1,3},{2,0},{3,1},{4,6},{5,7},{6,4},{7,5},{8,10},{9,11},{10,... | collective-permute-start | bytes 786440 | tf_op jit(solution)/shard_map/ppermute | solution.py:43
  109.4 30.4 %collective-permute-start.18 = (bf16[64,2048]{1,0:T(8,128)(2,1)S(1)}, bf16[64,2048]{1,0:T(8,128)(2,1)S(1)}, u32[]{:S(2)}, u32[]{:S(2)}) collective-permute-start(bf16[64,2048]{1,0:T(8,128)(2,1)S(1)} %get-tuple-element.35), channel_id=1, source_target_pairs={{0,2},{1,3},{2,0},{3,1},{4,6},{5,7},{6,4},{7,5},{8,10},{9,11},{10,... | collective-permute-start | bytes 786440 | tf_op jit(solution)/shard_map/ppermute | solution.py:43
  110.5 34.8 %collective-permute-start.19 = (bf16[64,2048]{1,0:T(8,128)(2,1)S(1)}, bf16[64,2048]{1,0:T(8,128)(2,1)S(1)}, u32[]{:S(2)}, u32[]{:S(2)}) collective-permute-start(bf16[64,2048]{1,0:T(8,128)(2,1)S(1)} %get-tuple-element.37), channel_id=1, source_target_pairs={{0,1},{1,2},{2,3},{3,0},{4,5},{5,6},{6,7},{7,4},{8,9},{9,10},{10,1... | collective-permute-start | bytes 786440 | tf_op jit(solution)/shard_map/ppermute | solution.py:43
  111.9 35.5 %collective-permute-start.20 = (bf16[64,2048]{1,0:T(8,128)(2,1)S(1)}, bf16[64,2048]{1,0:T(8,128)(2,1)S(1)}, u32[]{:S(2)}, u32[]{:S(2)}) collective-permute-start(bf16[64,2048]{1,0:T(8,128)(2,1)S(1)} %get-tuple-element.36), channel_id=1, source_target_pairs={{0,3},{1,0},{2,1},{3,2},{4,7},{5,4},{6,5},{7,6},{8,11},{9,8},{10,9... | collective-permute-start | bytes 786440 | tf_op jit(solution)/shard_map/ppermute | solution.py:43

commit v3 on v2

--- a/solution.py
+++ b/solution.py
@@ -93,7 +93,13 @@
         query_refs = refs[:sources]
         key_ref, value_ref = refs[sources : sources + 2]
         out_refs = refs[sources + 2 : 2 * sources + 2]
-        list_block, list_pass, part_ref, top_ref, sum_ref = refs[2 * sources + 2 :]
+        list_block, list_pass, part_ref, top_ref, sum_ref, weight_ref = refs[2 * sources + 2 :]
+
+        def held_rows(ref, h, at):
+            return jnp.concatenate(
+                [ref[h * lanes + c, pl.ds(at, pass_rows), :] for c in range(lanes)], axis=1
+            )
+
         first = me_ref[0] * held
         lane = lax.broadcasted_iota(jnp.int32, (block_len, 128), 1)
         for source in range(sources):
@@ -122,34 +128,36 @@
                     for h in range(heads):
                         cols = slice(h * HD, (h + 1) * HD)
                         q = query_ref[pl.ds(block_at, block_len), cols]
-                        k, v = (
-                            jnp.concatenate(
-                                [
-                                    ref[h * lanes + c, pl.ds(pass_at, pass_rows), :]
-                                    for c in range(lanes)
-                                ],
-                                axis=1,
-                            )
-                            for ref in (key_ref, value_ref)
-                        )
+                        k = held_rows(key_ref, h, pass_at)
                         scores = lax.dot_general(
                             q, k, (((1,), (1,)), ((), ())), preferred_element_type=jnp.float32
                         ) * scale
                         top = jnp.max(scores, axis=1, keepdims=True)
                         exponent = jnp.exp(scores - top)
                         total = jnp.sum(exponent, axis=1, keepdims=True)
+                        weight_ref[slot, h] = exponent.astype(jnp.bfloat16)
+                        top_ref[slot, h] = jnp.broadcast_to(top, (block_len, 128))
+                        sum_ref[slot, h] = jnp.broadcast_to(total, (block_len, 128))
+                return carry
+
+            def weigh(i, carry):
+                for u in range(BATCH):
+                    slot = i * BATCH + u
+                    pass_at = pl.multiple_of(list_pass[slot] * pass_rows, pass_rows)
+                    for h in range(heads):
                         out = jnp.dot(
-                            exponent.astype(jnp.bfloat16), v, preferred_element_type=jnp.float32
+                            weight_ref[slot, h],
+                            held_rows(value_ref, h, pass_at),
+                            preferred_element_type=jnp.float32,
                         )
                         for c in range(lanes):
                             part_ref[slot, h * lanes + c] = out[
                                 :, c * 128 : (c + 1) * 128
                             ].astype(jnp.bfloat16)
-                        top_ref[slot, h] = jnp.broadcast_to(top, (block_len, 128))
-                        sum_ref[slot, h] = jnp.broadcast_to(total, (block_len, 128))
                 return carry
 
             lax.fori_loop(0, trips, batch, 0)
+            lax.fori_loop(0, trips, weigh, 0)
             tiles = []
             for block in range(blocks):
                 held_here = starts[block + 1] - starts[block]
@@ -203,6 +211,7 @@
             pltpu.VMEM((slots, head_width // 128, block_len, 128), jnp.bfloat16),
             pltpu.VMEM((slots, heads, block_len, 128), jnp.float32),
             pltpu.VMEM((slots, heads, block_len, 128), jnp.float32),
+            pltpu.VMEM((slots, heads, block_len, pass_rows), jnp.bfloat16),
         ],
         name="owner_attention",
     )(me, ids, *query_list, keys, values)

time: 150 us -> 124 us (0.83); the launches traced: 148 us -> 125 us
  Pallas kernels: 63.9 us -> 29.3 us
  starting transfers between devices: 18.8 us -> 28.2 us
  waiting for transfers between devices: 34.2 us -> 36.5 us
    pallas_call x2, Pallas kernels: 49.4 us -> 14.8 us  [owner_attention(): pl.pallas_call(kernel, out_shape=[jax.ShapeDtypeStruct((rows + extra, hea...]
    ppermute x21, starting transfers between devices: 18.8 us -> 28.2 us  [shifted(): lax.ppermute(value, axis, [(i, (i + step) % size) for i in range(size)])]
    ppermute x21, waiting for transfers between devices: 34.2 us -> 36.5 us  [shifted(): lax.ppermute(value, axis, [(i, (i + step) % size) for i in range(size)])]
  transfers between devices with their start and end apart: 21 -> 21, of which waited for: 7 -> 7; matrix products, arithmetic and copies ran while one was open for 16% -> 20% of each run, Pallas kernels for 43% -> 23%
where the time goes in v3:
time: 124 us; the launch traced here: 125 us
  waiting for transfers between devices  36.5 us (29%)
  Pallas kernels  29.3 us (24%)
  starting transfers between devices  28.2 us (23%)
  matrix products  14.9 us (12%)
  other arithmetic  10.7 us (9%)
  local copies, waits for them, and re-layouts  5.57 us (4%)
    ppermute x21, waiting for transfers between devices, shifted(): lax.ppermute(value, axis, [(i, (i + step) % size) for i in range(size)])  36.5 us
    ppermute x21, starting transfers between devices, shifted(): lax.ppermute(value, axis, [(i, (i + step) % size) for i in range(size)])  28.2 us
    pallas_call x2, Pallas kernels, owner_attention(): pl.pallas_call(kernel, out_shape=[jax.ShapeDtypeStruct((rows + extra, hea...  14.8 us
    pallas_call x1, Pallas kernels, passage_planes(): pl.pallas_call(kernel, grid=(total_rows // step_rows,), out_shape=[jax.Sh...  9.46 us
    pallas_call x2, Pallas kernels, merge_owners(): pl.pallas_call(kernel, out_shape=jax.ShapeDtypeStruct((rows, head_width),...  5.05 us
    dot_general x2, matrix products, local(): attn_term = jnp.dot(attended, attn_out, preferred_element_type=jnp.float32)  4.81 us
    slice x6, local copies, waits for them, and re-layouts, local(): q[shards * run, :ids.shape[1]]  3.9 us
    dot_general x2, matrix products, local(): jnp.dot(cut(activation, c), mix_out, preferred_element_type=jnp.float32)  3.53 us
  transfers between devices with their start and end apart: 21, of which 7 were waited for; matrix products, arithmetic and copies ran while one was open for 20% of the time, Pallas kernels for 23%

profile of v3, /device:TPU:9, one launch (start us, length us, event | category | flops | bytes accessed | tf_op | source)
XLA Modules:
  0.0 125.4 jit_solution(7261721120321927638)
XLA Ops:
  0.0 2.2 %fusion.4 = f32[512]{0:T(512)S(1)} fusion(bf16[512,2048]{1,0:T(8,128)(2,1)} %param.16), kind=kLoop, calls=%fused_computation.6 | loop fusion | flops 3145216 | bytes 2099200 | tf_op jit(solution)/shard_map/reduce_sum | solution.py:18
  2.4 3.0 %fusion.13 = bf16[512,512]{1,0:T(8,128)(2,1)S(1)} fusion(bf16[2048,512]{1,0:T(8,128)(2,1)} %param.27, bf16[512,2048]{1,0:T(8,128)(2,1)S(1)} %copy-done.2, f32[2048]{0:T(1024)} %param.25, f32[512]{0:T(512)S(1)} %add_rsqrt_fusion.1), kind=kOutput, calls=%fused_computation.46 | convolution fusion | flops 1078198272 | bytes 4728832 | tf_op jit(solution)/shard_map/dot_general | solution.py:308
  5.6 1.8 %collective-permute-start.3 = (bf16[272,512]{1,0:T(8,128)(2,1)S(1)}, bf16[272,512]{1,0:T(8,128)(2,1)}, u32[]{:S(2)}, u32[]{:S(2)}) collective-permute-start(bf16[272,512]{1,0:T(8,128)(2,1)S(1)} %fusion.90.refs_0_), channel_id=1, source_target_pairs={{0,4},{4,8},{8,12},{12,0},{1,5},{5,9},{9,13},{13,1},{2,6},{6,10},{... | collective-permute-start | bytes 835592 | tf_op jit(solution)/shard_map/ppermute | solution.py:43
  7.8 2.8 %fusion.18 = f32[512,256]{1,0:T(8,128)S(1)} fusion(bf16[2048,256]{1,0:T(8,128)(2,1)} %param.21, bf16[512,2048]{1,0:T(8,128)(2,1)} %param.16, f32[2048]{0:T(1024)S(1)} %copy-done.15, f32[512]{0:T(512)S(1)} %add_rsqrt_fusion.1), kind=kOutput, calls=%fused_computation.51 | convolution fusion | flops 541458432 | bytes 3680256 | tf_op jit(solution)/shard_map/dot_general | solution.py:330
  10.6 0.8 bitcast_convert_fusion
  11.4 2.9 %fusion.94 = (f32[4,128]{1,0:T(4,128)S(1)}, f32[4,128]{1,0:T(4,128)S(1)}, f32[4,128,256]{2,1,0:T(8,128)}) fusion(f32[256]{0:T(256)S(1)} %bitcast.129, f32[256]{0:T(256)S(1)} %bitcast.130, f32[256]{0:T(256)S(1)} %bitcast.101, f32[256]{0:T(256)S(1)} %bitcast.102, f32[256]{0:T(256)S(1)} %bitcast.103, f32[256]{0:T(256)S(1)} %bitcast.104, f32[256]{0:T(256)S(1)} %bitcast.105, ...), kind=kLoop, calls=%fused_computation.178 | loop fusion | flops 8387584 | bytes 1084416 | tf_op jit(solution)/shard_map/reduce_sum | solution.py:335
  14.4 1.3 %collective-permute-start = (f32[2,512]{1,0:T(2,128)S(1)}, f32[2,512]{1,0:T(2,128)S(1)}, u32[]{:S(2)}, u32[]{:S(2)}) collective-permute-start(f32[2,512]{1,0:T(2,128)S(1)} %pad_maximum_fusion.1), channel_id=1, source_target_pairs={{0,1},{1,2},{2,3},{3,0},{4,5},{5,6},{6,7},{7,4},{8,9},{9,10},{10,1... | collective-permute-start | bytes 12296 | tf_op jit(solution)/shard_map/ppermute | solution.py:43
  15.7 1.1 collective-permute-start.1
  16.8 1.4 %collective-permute-start.2 = (f32[2,512]{1,0:T(2,128)S(1)}, f32[2,512]{1,0:T(2,128)S(1)}, u32[]{:S(2)}, u32[]{:S(2)}) collective-permute-start(f32[2,512]{1,0:T(2,128)S(1)} %pad_maximum_fusion.1), channel_id=1, source_target_pairs={{0,3},{1,0},{2,1},{3,2},{4,7},{5,4},{6,5},{7,6},{8,11},{9,8},{10,9... | collective-permute-start | bytes 12296 | tf_op jit(solution)/shard_map/ppermute | solution.py:43
  18.3 0.8 fusion.91.refs_0_
  19.0 9.5 %passage_planes.1 = (bf16[4,1024,128]{2,1,0:T(8,128)(2,1)}, bf16[4,1024,128]{2,1,0:T(8,128)(2,1)}) custom-call(bf16[1024,2048]{1,0:T(8,128)(2,1)} %bitcast.83, f32[1,2048]{1,0:T(1,128)} %bitcast.99, bf16[2048,512]{1,0:T(8,128)(2,1)} %key_w.1, bf16[2048,512]{1,0:T(8,128)(2,1)} %value_w.1), custom_call_target="tpu_custom_call" | custom-call | tf_op jit(solution)/shard_map/passage_planes/pallas_call | solution.py:62
  28.5 1.1 collective-permute-start.5
  29.7 0.7 collective-permute-start.12
  30.3 1.2 collective-permute-start.13
  31.8 1.3 %multiply_convert_fusion = bf16[4,2,64,256]{3,2,1,0:T(8,128)(2,1)S(1)} fusion(f32[4,2,64,256]{3,2,1,0:T(8,128)} %bitcast.88, f32[256]{0:T(256)S(1)} %copy-done.13, f32[4,2,64]{2,1,0:T(2,128)S(1)} %add_rsqrt_fusion, f32[4,2,64]{2,1,0:T(2,128)S(1)} %div.25), kind=kLoop, calls=%fused_computation.125 | loop fusion | flops 1048576 | bytes 791552 | tf_op jit(solution)/shard_map/convert_element_type | solution.py:356
  33.1 1.8 %fusion.98 = f32[256,2048]{1,0:T(8,128)} fusion(bf16[256,256]{1,0:T(8,128)(2,1)S(1)} %bitcast.93, bf16[256,2048]{1,0:T(8,128)(2,1)S(1)} %copy-done.1), kind=kOutput, calls=%fused_computation.182 | convolution fusion | flops 268435456 | bytes 3276800 | tf_op jit(solution)/shard_map/dot_general | solution.py:360
  34.9 0.6 slice.310
  35.5 0.7 slice.311
  36.2 0.6 collective-permute-done.5.refs_3_
  36.8 0.7 slice.312
  37.4 0.6 maximum_convert_fusion.ids_ref
  38.0 7.4 %owner_attention.2 = (bf16[272,512]{1,0:T(8,128)(2,1)}, bf16[272,512]{1,0:T(8,128)(2,1)}, bf16[272,512]{1,0:T(8,128)(2,1)}, bf16[272,512]{1,0:T(8,128)(2,1)}) custom-call(s32[1]{0:T(128)} %bitcast.37.me_ref, s32[4,16]{1,0:T(4,128)} %maximum_convert_fusion.ids_ref, bf16[272,512]{1,0:T(8,128)(2,1)} %copy-done.4, ...), custom_call_target="tpu_custom_call" | custom-call | tf_op jit(solution)/shard_map/owner_attention/pallas_call | solution.py:203
  45.8 5.4 %collective-permute-start.7 = (bf16[272,512]{1,0:T(8,128)(2,1)}, bf16[272,512]{1,0:T(8,128)(2,1)}, u32[]{:S(2)}, u32[]{:S(2)}) collective-permute-start(bf16[272,512]{1,0:T(8,128)(2,1)} %get-tuple-element.19), channel_id=1, source_target_pairs={{0,8},{4,12},{8,0},{12,4},{1,9},{5,13},{9,1},{13,5},{2,10},{6,14},... | collective-permute-start | bytes 835592 | tf_op jit(solution)/shard_map/ppermute | solution.py:43
  51.2 2.0 %collective-permute-start.8 = (bf16[272,512]{1,0:T(8,128)(2,1)}, bf16[272,512]{1,0:T(8,128)(2,1)}, u32[]{:S(2)}, u32[]{:S(2)}) collective-permute-start(bf16[272,512]{1,0:T(8,128)(2,1)} %get-tuple-element.20), channel_id=1, source_target_pairs={{0,4},{4,8},{8,12},{12,0},{1,5},{5,9},{9,13},{13,1},{2,6},{6,10},{... | collective-permute-start | bytes 835592 | tf_op jit(solution)/shard_map/ppermute | solution.py:43
  53.2 1.8 %fusion.99 = f32[256,2048]{1,0:T(8,128)} fusion(bf16[256,256]{1,0:T(8,128)(2,1)S(1)} %bitcast.92, bf16[256,2048]{1,0:T(8,128)(2,1)S(1)} %copy-done.1), kind=kOutput, calls=%fused_computation.183 | convolution fusion | flops 268435456 | bytes 3276800 | tf_op jit(solution)/shard_map/dot_general | solution.py:360
  55.0 0.7 slice.316
  55.6 0.7 slice.317
  56.3 0.6 slice.318
  56.9 0.6 maximum_convert_fusion.1.ids_ref
  57.5 7.4 %owner_attention.3 = (bf16[272,512]{1,0:T(8,128)(2,1)}, bf16[272,512]{1,0:T(8,128)(2,1)}, bf16[272,512]{1,0:T(8,128)(2,1)}, bf16[272,512]{1,0:T(8,128)(2,1)}) custom-call(s32[1]{0:T(128)} %bitcast.37.me_ref, s32[4,16]{1,0:T(4,128)} %maximum_convert_fusion.1.ids_ref, bf16[272,512]{1,0:T(8,128)(2,1)} %fusion.91.refs_0_, ...), custom_call_target="tpu_custom_call" | custom-call | tf_op jit(solution)/shard_map/owner_attention/pallas_call | solution.py:203
  64.9 3.9 %collective-permute-start.16 = (bf16[272,512]{1,0:T(8,128)(2,1)}, bf16[272,512]{1,0:T(8,128)(2,1)}, u32[]{:S(2)}, u32[]{:S(2)}) collective-permute-start(bf16[272,512]{1,0:T(8,128)(2,1)} %get-tuple-element.23), channel_id=1, source_target_pairs={{0,8},{4,12},{8,0},{12,4},{1,9},{5,13},{9,1},{13,5},{2,10},{6,14},... | collective-permute-start | bytes 835592 | tf_op jit(solution)/shard_map/ppermute | solution.py:43
  68.8 2.0 %collective-permute-start.17 = (bf16[272,512]{1,0:T(8,128)(2,1)}, bf16[272,512]{1,0:T(8,128)(2,1)}, u32[]{:S(2)}, u32[]{:S(2)}) collective-permute-start(bf16[272,512]{1,0:T(8,128)(2,1)} %get-tuple-element.24), channel_id=1, source_target_pairs={{0,4},{4,8},{8,12},{12,0},{1,5},{5,9},{9,13},{13,1},{2,6},{6,10},{... | collective-permute-start | bytes 835592 | tf_op jit(solution)/shard_map/ppermute | solution.py:43
  70.9 2.5 %merge_owners.2 = bf16[256,512]{1,0:T(8,128)(2,1)} custom-call(bf16[272,512]{1,0:T(8,128)(2,1)} %get-tuple-element.17.refs_0_, bf16[272,512]{1,0:T(8,128)(2,1)} %copy-done.5, bf16[272,512]{1,0:T(8,128)(2,1)} %collective-permute-done.7.refs_2_, bf16[272,512]{1,0:T(8,128)(2,1)} %collective-permute-done.8.refs_3_), custom_call_target="tpu_custom_call" | custom-call | tf_op jit(solution)/shard_map/merge_owners/pallas_call | solution.py:263
  73.4 2.4 %fusion.7 = bf16[256,2048]{1,0:T(8,128)(2,1)S(1)} fusion(f32[256,2048]{1,0:T(8,128)} %fusion.98, bf16[256,512]{1,0:T(8,128)(2,1)} %merge_owners.2, bf16[512,2048]{1,0:T(8,128)(2,1)S(1)} %copy-done, f32[2048]{0:T(1024)S(1)} %copy-done.7), kind=kOutput, calls=%fused_computation.11 | convolution fusion | flops 538443776 | bytes 5513216 | tf_op jit(solution)/shard_map/dot_general | solution.py:361
  75.8 0.9 dynamic-slice_bitcast_fusion.5
  76.9 1.3 %collective-permute-start.11 = (bf16[64,2048]{1,0:T(8,128)(2,1)}, bf16[64,2048]{1,0:T(8,128)(2,1)}, u32[]{:S(2)}, u32[]{:S(2)}) collective-permute-start(bf16[64,2048]{1,0:T(8,128)(2,1)} %get-tuple-element.33), channel_id=1, source_target_pairs={{0,3},{1,0},{2,1},{3,2},{4,7},{5,4},{6,5},{7,6},{8,11},{9,8},{10,9... | collective-permute-start | bytes 786440 | tf_op jit(solution)/shard_map/ppermute | solution.py:43
  78.2 1.7 %collective-permute-start.9 = (bf16[64,2048]{1,0:T(8,128)(2,1)}, bf16[64,2048]{1,0:T(8,128)(2,1)}, u32[]{:S(2)}, u32[]{:S(2)}) collective-permute-start(bf16[64,2048]{1,0:T(8,128)(2,1)} %get-tuple-element.32), channel_id=1, source_target_pairs={{0,2},{1,3},{2,0},{3,1},{4,6},{5,7},{6,4},{7,5},{8,10},{9,11},{10,... | collective-permute-start | bytes 786440 | tf_op jit(solution)/shard_map/ppermute | solution.py:43
  79.9 1.1 collective-permute-done.17.refs_3_
  81.0 2.5 %merge_owners.3 = bf16[256,512]{1,0:T(8,128)(2,1)} custom-call(bf16[272,512]{1,0:T(8,128)(2,1)} %get-tuple-element.21.refs_0_, bf16[272,512]{1,0:T(8,128)(2,1)} %collective-permute-done.15.refs_1_, bf16[272,512]{1,0:T(8,128)(2,1)} %collective-permute-done.16.refs_2_, bf16[272,512]{1,0:T(8,128)(2,1)} %collective-permute-done.17.refs_3_), custom_call_target="tpu_custom_call" | custom-call | tf_op jit(solution)/shard_map/merge_owners/pallas_call | solution.py:263
  83.5 2.4 %fusion.8 = bf16[256,2048]{1,0:T(8,128)(2,1)S(1)} fusion(f32[256,2048]{1,0:T(8,128)} %fusion.99, bf16[256,512]{1,0:T(8,128)(2,1)} %merge_owners.3, bf16[512,2048]{1,0:T(8,128)(2,1)S(1)} %copy-done, f32[2048]{0:T(1024)S(1)} %copy-done.7), kind=kOutput, calls=%fused_computation.12 | convolution fusion | flops 538443776 | bytes 5513216 | tf_op jit(solution)/shard_map/dot_general | solution.py:361
  86.1 2.2 %collective-permute-start.19 = (bf16[64,2048]{1,0:T(8,128)(2,1)S(1)}, bf16[64,2048]{1,0:T(8,128)(2,1)S(1)}, u32[]{:S(2)}, u32[]{:S(2)}) collective-permute-start(bf16[64,2048]{1,0:T(8,128)(2,1)S(1)} %get-tuple-element.37), channel_id=1, source_target_pairs={{0,1},{1,2},{2,3},{3,0},{4,5},{5,6},{6,7},{7,4},{8,9},{9,10},{10,1... | collective-permute-start | bytes 786440 | tf_op jit(solution)/shard_map/ppermute | solution.py:43
  88.5 2.3 %collective-permute-done.11 = bf16[64,2048]{1,0:T(8,128)(2,1)} collective-permute-done((bf16[64,2048]{1,0:T(8,128)(2,1)}, bf16[64,2048]{1,0:T(8,128)(2,1)}, u32[]{:S(2)}, u32[]{:S(2)}) %collective-permute-start.11) | collective-permute-done | bytes 262176 | tf_op jit(solution)/shard_map/ppermute | solution.py:43
  90.8 14.9 %collective-permute-done.9 = bf16[64,2048]{1,0:T(8,128)(2,1)} collective-permute-done((bf16[64,2048]{1,0:T(8,128)(2,1)}, bf16[64,2048]{1,0:T(8,128)(2,1)}, u32[]{:S(2)}, u32[]{:S(2)}) %collective-permute-start.9) | collective-permute-done | bytes 262176 | tf_op jit(solution)/shard_map/ppermute | solution.py:43
  105.8 1.2 fusion.89
  106.9 10.0 %collective-permute-done.18 = bf16[64,2048]{1,0:T(8,128)(2,1)S(1)} collective-permute-done((bf16[64,2048]{1,0:T(8,128)(2,1)S(1)}, bf16[64,2048]{1,0:T(8,128)(2,1)S(1)}, u32[]{:S(2)}, u32[]{:S(2)}) %collective-permute-start.18) | collective-permute-done | bytes 262176 | tf_op jit(solution)/shard_map/ppermute | solution.py:43
  116.9 5.2 %collective-permute-done.19 = bf16[64,2048]{1,0:T(8,128)(2,1)S(1)} collective-permute-done((bf16[64,2048]{1,0:T(8,128)(2,1)S(1)}, bf16[64,2048]{1,0:T(8,128)(2,1)S(1)}, u32[]{:S(2)}, u32[]{:S(2)}) %collective-permute-start.19) | collective-permute-done | bytes 262176 | tf_op jit(solution)/shard_map/ppermute | solution.py:43
  122.1 2.3 %collective-permute-done.20 = bf16[64,2048]{1,0:T(8,128)(2,1)S(1)} collective-permute-done((bf16[64,2048]{1,0:T(8,128)(2,1)S(1)}, bf16[64,2048]{1,0:T(8,128)(2,1)S(1)}, u32[]{:S(2)}, u32[]{:S(2)}) %collective-permute-start.20) | collective-permute-done | bytes 262176 | tf_op jit(solution)/shard_map/ppermute | solution.py:43
  124.5 0.8 pad_maximum_fusion
  (72 shorter events, 2.1 us)
Async XLA Ops:
  0.0 73.4 %copy-start = (bf16[512,2048]{1,0:T(8,128)(2,1)S(1)}, bf16[512,2048]{1,0:T(8,128)(2,1)}, u32[]{:S(2)}) copy-start(bf16[512,2048]{1,0:T(8,128)(2,1)} %param.30) | copy-start | bytes 6291460
  0.0 2.4 %copy-start.2 = (bf16[512,2048]{1,0:T(8,128)(2,1)S(1)}, bf16[512,2048]{1,0:T(8,128)(2,1)}, u32[]{:S(2)}) copy-start(bf16[512,2048]{1,0:T(8,128)(2,1)} %param.16) | copy-start | bytes 6291460
  2.4 3.0 %copy-start.12 = (s32[8,4]{0,1:T(4,128)S(1)}, s32[8,4]{0,1:T(4,128)}, u32[]{:S(2)}) copy-start(s32[8,4]{0,1:T(4,128)} %param.18) | copy-start | bytes 388
  2.4 5.3 %copy-start.6 = (bf16[31,256]{1,0:T(8,128)(2,1)S(1)}, bf16[31,256]{1,0:T(8,128)(2,1)}, u32[]{:S(2)}) copy-start(bf16[31,256]{1,0:T(8,128)(2,1)} %param.22) | copy-start | bytes 47620
  2.4 5.4 %copy-start.15 = (f32[2048]{0:T(1024)S(1)}, f32[2048]{0:T(1024)}, u32[]{:S(2)}) copy-start(f32[2048]{0:T(1024)} %param.19) | copy-start | bytes 24580
  5.6 2.2 %copy-start.8 = (bf16[1,16]{1,0:T(2,128)(2,1)}, bf16[1,16]{1,0:T(2,128)(2,1)S(1)}, u32[]{:S(2)}) copy-start(bf16[1,16]{1,0:T(2,128)(2,1)S(1)} %convert_element_type.481) | copy-start | bytes 100
  5.6 22.9 %copy-start.4 = (bf16[272,512]{1,0:T(8,128)(2,1)}, bf16[272,512]{1,0:T(8,128)(2,1)S(1)}, u32[]{:S(2)}) copy-start(bf16[272,512]{1,0:T(8,128)(2,1)S(1)} %fusion.90.refs_0_) | copy-start | bytes 835588
  5.6 29.2 %collective-permute-start.3 = (bf16[272,512]{1,0:T(8,128)(2,1)S(1)}, bf16[272,512]{1,0:T(8,128)(2,1)}, u32[]{:S(2)}, u32[]{:S(2)}) collective-permute-start(bf16[272,512]{1,0:T(8,128)(2,1)S(1)} %fusion.90.refs_0_), channel_id=1, source_target_pairs={{0,4},{4,8},{8,12},{12,0},{1,5},{5,9},{9,13},{13,1},{2,6},{6,10},{... | collective-permute-start | bytes 835592 | tf_op jit(solution)/shard_map/ppermute | solution.py:43
  7.5 28.0 %collective-permute-start.4 = (bf16[272,512]{1,0:T(8,128)(2,1)S(1)}, bf16[272,512]{1,0:T(8,128)(2,1)}, u32[]{:S(2)}, u32[]{:S(2)}) collective-permute-start(bf16[272,512]{1,0:T(8,128)(2,1)S(1)} %fusion.90.refs_0_), channel_id=1, source_target_pairs={{0,8},{4,12},{8,0},{12,4},{1,9},{5,13},{9,1},{13,5},{2,10},{6,14},... | collective-permute-start | bytes 835592 | tf_op jit(solution)/shard_map/ppermute | solution.py:43
  7.8 2.8 %copy-start.3 = (bf16[512,2048]{1,0:T(8,128)(2,1)S(1)}, bf16[512,2048]{1,0:T(8,128)(2,1)}, u32[]{:S(2)}) copy-start(bf16[512,2048]{1,0:T(8,128)(2,1)} %param.16) | copy-start | bytes 6291460
  7.8 2.8 %copy-start.14 = (bf16[2048,256]{1,0:T(8,128)(2,1)S(1)}, bf16[2048,256]{1,0:T(8,128)(2,1)}, u32[]{:S(2)}) copy-start(bf16[2048,256]{1,0:T(8,128)(2,1)} %param.20) | copy-start | bytes 3145732
  14.4 14.1 %collective-permute-start = (f32[2,512]{1,0:T(2,128)S(1)}, f32[2,512]{1,0:T(2,128)S(1)}, u32[]{:S(2)}, u32[]{:S(2)}) collective-permute-start(f32[2,512]{1,0:T(2,128)S(1)} %pad_maximum_fusion.1), channel_id=1, source_target_pairs={{0,1},{1,2},{2,3},{3,0},{4,5},{5,6},{6,7},{7,4},{8,9},{9,10},{10,1... | collective-permute-start | bytes 12296 | tf_op jit(solution)/shard_map/ppermute | solution.py:43
  15.7 14.0 %collective-permute-start.1 = (f32[2,512]{1,0:T(2,128)S(1)}, f32[2,512]{1,0:T(2,128)S(1)}, u32[]{:S(2)}, u32[]{:S(2)}) collective-permute-start(f32[2,512]{1,0:T(2,128)S(1)} %pad_maximum_fusion.1), channel_id=1, source_target_pairs={{0,2},{1,3},{2,0},{3,1},{4,6},{5,7},{6,4},{7,5},{8,10},{9,11},{10,... | collective-permute-start | bytes 12296 | tf_op jit(solution)/shard_map/ppermute | solution.py:43
  16.8 13.5 %collective-permute-start.2 = (f32[2,512]{1,0:T(2,128)S(1)}, f32[2,512]{1,0:T(2,128)S(1)}, u32[]{:S(2)}, u32[]{:S(2)}) collective-permute-start(f32[2,512]{1,0:T(2,128)S(1)} %pad_maximum_fusion.1), channel_id=1, source_target_pairs={{0,3},{1,0},{2,1},{3,2},{4,7},{5,4},{6,5},{7,6},{8,11},{9,8},{10,9... | collective-permute-start | bytes 12296 | tf_op jit(solution)/shard_map/ppermute | solution.py:43
  18.3 0.8 copy-start.10
  19.0 12.7 %copy-start.13 = (f32[256]{0:T(256)S(1)}, f32[256]{0:T(256)}, u32[]{:S(2)}) copy-start(f32[256]{0:T(256)} %param.23) | copy-start | bytes 3076
  28.5 4.6 %copy-start.1 = (bf16[256,2048]{1,0:T(8,128)(2,1)S(1)}, bf16[256,2048]{1,0:T(8,128)(2,1)}, u32[]{:S(2)}) copy-start(bf16[256,2048]{1,0:T(8,128)(2,1)} %param.24) | copy-start | bytes 3145732
  28.5 8.2 %collective-permute-start.5 = (bf16[272,512]{1,0:T(8,128)(2,1)S(1)}, bf16[272,512]{1,0:T(8,128)(2,1)}, u32[]{:S(2)}, u32[]{:S(2)}) collective-permute-start(bf16[272,512]{1,0:T(8,128)(2,1)S(1)} %fusion.90.refs_0_), channel_id=1, source_target_pairs={{0,12},{4,0},{8,4},{12,8},{1,13},{5,1},{9,5},{13,9},{2,14},{6,2},{... | collective-permute-start | bytes 835592 | tf_op jit(solution)/shard_map/ppermute | solution.py:43
  29.7 21.5 %collective-permute-start.12 = (bf16[272,512]{1,0:T(8,128)(2,1)}, bf16[272,512]{1,0:T(8,128)(2,1)}, u32[]{:S(2)}, u32[]{:S(2)}) collective-permute-start(bf16[272,512]{1,0:T(8,128)(2,1)} %fusion.91.refs_0_), channel_id=1, source_target_pairs={{0,4},{4,8},{8,12},{12,0},{1,5},{5,9},{9,13},{13,1},{2,6},{6,10},{... | collective-permute-start | bytes 835592 | tf_op jit(solution)/shard_map/ppermute | solution.py:43
  30.3 25.3 %collective-permute-start.13 = (bf16[272,512]{1,0:T(8,128)(2,1)}, bf16[272,512]{1,0:T(8,128)(2,1)}, u32[]{:S(2)}, u32[]{:S(2)}) collective-permute-start(bf16[272,512]{1,0:T(8,128)(2,1)} %fusion.91.refs_0_), channel_id=1, source_target_pairs={{0,8},{4,12},{8,0},{12,4},{1,9},{5,13},{9,1},{13,5},{2,10},{6,14},... | collective-permute-start | bytes 835592 | tf_op jit(solution)/shard_map/ppermute | solution.py:43
  33.1 4.3 %copy-start.9 = (bf16[1,16]{1,0:T(2,128)(2,1)S(1)}, bf16[1,16]{1,0:T(2,128)(2,1)}, u32[]{:S(2)}) copy-start(bf16[1,16]{1,0:T(2,128)(2,1)} %copy-done.8) | copy-start | bytes 100
  34.9 21.4 %collective-permute-start.14 = (bf16[272,512]{1,0:T(8,128)(2,1)}, bf16[272,512]{1,0:T(8,128)(2,1)}, u32[]{:S(2)}, u32[]{:S(2)}) collective-permute-start(bf16[272,512]{1,0:T(8,128)(2,1)} %fusion.91.refs_0_), channel_id=1, source_target_pairs={{0,12},{4,0},{8,4},{12,8},{1,13},{5,1},{9,5},{13,9},{2,14},{6,2},{... | collective-permute-start | bytes 835592 | tf_op jit(solution)/shard_map/ppermute | solution.py:43
  45.4 11.5 %copy-start.11 = (bf16[1,16]{1,0:T(2,128)(2,1)S(1)}, bf16[1,16]{1,0:T(2,128)(2,1)}, u32[]{:S(2)}) copy-start(bf16[1,16]{1,0:T(2,128)(2,1)} %copy-done.10) | copy-start | bytes 100
  45.4 23.4 %collective-permute-start.6 = (bf16[272,512]{1,0:T(8,128)(2,1)}, bf16[272,512]{1,0:T(8,128)(2,1)S(1)}, u32[]{:S(2)}, u32[]{:S(2)}) collective-permute-start(bf16[272,512]{1,0:T(8,128)(2,1)} %get-tuple-element.18), channel_id=1, source_target_pairs={{0,12},{4,0},{8,4},{12,8},{1,13},{5,1},{9,5},{13,9},{2,14},{6,2},{... | collective-permute-start | bytes 835592 | tf_op jit(solution)/shard_map/ppermute | solution.py:43
  45.8 25.1 %collective-permute-start.7 = (bf16[272,512]{1,0:T(8,128)(2,1)}, bf16[272,512]{1,0:T(8,128)(2,1)}, u32[]{:S(2)}, u32[]{:S(2)}) collective-permute-start(bf16[272,512]{1,0:T(8,128)(2,1)} %get-tuple-element.19), channel_id=1, source_target_pairs={{0,8},{4,12},{8,0},{12,4},{1,9},{5,13},{9,1},{13,5},{2,10},{6,14},... | collective-permute-start | bytes 835592 | tf_op jit(solution)/shard_map/ppermute | solution.py:43
  51.2 19.6 %collective-permute-start.8 = (bf16[272,512]{1,0:T(8,128)(2,1)}, bf16[272,512]{1,0:T(8,128)(2,1)}, u32[]{:S(2)}, u32[]{:S(2)}) collective-permute-start(bf16[272,512]{1,0:T(8,128)(2,1)} %get-tuple-element.20), channel_id=1, source_target_pairs={{0,4},{4,8},{8,12},{12,0},{1,5},{5,9},{9,13},{13,1},{2,6},{6,10},{... | collective-permute-start | bytes 835592 | tf_op jit(solution)/shard_map/ppermute | solution.py:43
  57.5 15.9 %copy-start.7 = (f32[2048]{0:T(1024)S(1)}, f32[2048]{0:T(1024)}, u32[]{:S(2)}) copy-start(f32[2048]{0:T(1024)} %param.31) | copy-start | bytes 24580
  64.9 13.3 %collective-permute-start.15 = (bf16[272,512]{1,0:T(8,128)(2,1)}, bf16[272,512]{1,0:T(8,128)(2,1)}, u32[]{:S(2)}, u32[]{:S(2)}) collective-permute-start(bf16[272,512]{1,0:T(8,128)(2,1)} %get-tuple-element.22), channel_id=1, source_target_pairs={{0,12},{4,0},{8,4},{12,8},{1,13},{5,1},{9,5},{13,9},{2,14},{6,2},{... | collective-permute-start | bytes 835592 | tf_op jit(solution)/shard_map/ppermute | solution.py:43
  64.9 14.9 %collective-permute-start.16 = (bf16[272,512]{1,0:T(8,128)(2,1)}, bf16[272,512]{1,0:T(8,128)(2,1)}, u32[]{:S(2)}, u32[]{:S(2)}) collective-permute-start(bf16[272,512]{1,0:T(8,128)(2,1)} %get-tuple-element.23), channel_id=1, source_target_pairs={{0,8},{4,12},{8,0},{12,4},{1,9},{5,13},{9,1},{13,5},{2,10},{6,14},... | collective-permute-start | bytes 835592 | tf_op jit(solution)/shard_map/ppermute | solution.py:43
  68.8 2.0 %copy-start.5 = (bf16[272,512]{1,0:T(8,128)(2,1)}, bf16[272,512]{1,0:T(8,128)(2,1)S(1)}, u32[]{:S(2)}) copy-start(bf16[272,512]{1,0:T(8,128)(2,1)S(1)} %collective-permute-done.6.refs_1_) | copy-start | bytes 835588
  68.8 12.2 %collective-permute-start.17 = (bf16[272,512]{1,0:T(8,128)(2,1)}, bf16[272,512]{1,0:T(8,128)(2,1)}, u32[]{:S(2)}, u32[]{:S(2)}) collective-permute-start(bf16[272,512]{1,0:T(8,128)(2,1)} %get-tuple-element.24), channel_id=1, source_target_pairs={{0,4},{4,8},{8,12},{12,0},{1,5},{5,9},{9,13},{13,1},{2,6},{6,10},{... | collective-permute-start | bytes 835592 | tf_op jit(solution)/shard_map/ppermute | solution.py:43
  76.7 11.6 %collective-permute-start.10 = (bf16[64,2048]{1,0:T(8,128)(2,1)}, bf16[64,2048]{1,0:T(8,128)(2,1)S(1)}, u32[]{:S(2)}, u32[]{:S(2)}) collective-permute-start(bf16[64,2048]{1,0:T(8,128)(2,1)} %get-tuple-element.34), channel_id=1, source_target_pairs={{0,1},{1,2},{2,3},{3,0},{4,5},{5,6},{6,7},{7,4},{8,9},{9,10},{10,1... | collective-permute-start | bytes 786440 | tf_op jit(solution)/shard_map/ppermute | solution.py:43
  76.9 14.0 %collective-permute-start.11 = (bf16[64,2048]{1,0:T(8,128)(2,1)}, bf16[64,2048]{1,0:T(8,128)(2,1)}, u32[]{:S(2)}, u32[]{:S(2)}) collective-permute-start(bf16[64,2048]{1,0:T(8,128)(2,1)} %get-tuple-element.33), channel_id=1, source_target_pairs={{0,3},{1,0},{2,1},{3,2},{4,7},{5,4},{6,5},{7,6},{8,11},{9,8},{10,9... | collective-permute-start | bytes 786440 | tf_op jit(solution)/shard_map/ppermute | solution.py:43
  78.2 27.6 %collective-permute-start.9 = (bf16[64,2048]{1,0:T(8,128)(2,1)}, bf16[64,2048]{1,0:T(8,128)(2,1)}, u32[]{:S(2)}, u32[]{:S(2)}) collective-permute-start(bf16[64,2048]{1,0:T(8,128)(2,1)} %get-tuple-element.32), channel_id=1, source_target_pairs={{0,2},{1,3},{2,0},{3,1},{4,6},{5,7},{6,4},{7,5},{8,10},{9,11},{10,... | collective-permute-start | bytes 786440 | tf_op jit(solution)/shard_map/ppermute | solution.py:43
  86.0 30.9 %collective-permute-start.18 = (bf16[64,2048]{1,0:T(8,128)(2,1)S(1)}, bf16[64,2048]{1,0:T(8,128)(2,1)S(1)}, u32[]{:S(2)}, u32[]{:S(2)}) collective-permute-start(bf16[64,2048]{1,0:T(8,128)(2,1)S(1)} %get-tuple-element.35), channel_id=1, source_target_pairs={{0,2},{1,3},{2,0},{3,1},{4,6},{5,7},{6,4},{7,5},{8,10},{9,11},{10,... | collective-permute-start | bytes 786440 | tf_op jit(solution)/shard_map/ppermute | solution.py:43
  86.1 36.0 %collective-permute-start.19 = (bf16[64,2048]{1,0:T(8,128)(2,1)S(1)}, bf16[64,2048]{1,0:T(8,128)(2,1)S(1)}, u32[]{:S(2)}, u32[]{:S(2)}) collective-permute-start(bf16[64,2048]{1,0:T(8,128)(2,1)S(1)} %get-tuple-element.37), channel_id=1, source_target_pairs={{0,1},{1,2},{2,3},{3,0},{4,5},{5,6},{6,7},{7,4},{8,9},{9,10},{10,1... | collective-permute-start | bytes 786440 | tf_op jit(solution)/shard_map/ppermute | solution.py:43
  88.3 36.1 %collective-permute-start.20 = (bf16[64,2048]{1,0:T(8,128)(2,1)S(1)}, bf16[64,2048]{1,0:T(8,128)(2,1)S(1)}, u32[]{:S(2)}, u32[]{:S(2)}) collective-permute-start(bf16[64,2048]{1,0:T(8,128)(2,1)S(1)} %get-tuple-element.36), channel_id=1, source_target_pairs={{0,3},{1,0},{2,1},{3,2},{4,7},{5,4},{6,5},{7,6},{8,11},{9,8},{10,9... | collective-permute-start | bytes 786440 | tf_op jit(solution)/shard_map/ppermute | solution.py:43
